TPU v7x, 32 devices: a whole 2x2x4 slice. The times are simulated.
32 devices in a mesh: sp: 8 (over z, y), tp: 4 (over x, core).
Axes of the slice: x: 2, y: 2, z: 4, core: 2. Of those that a mesh axis runs over, the one named last changes fastest.
Arguments:
- memory_queries: bfloat16 [4096, 1024], P('sp', 'tp'), may hold values from -8 to 8
- memory_keys: bfloat16 [4096, 1024], P('sp', 'tp'), may hold values from -8 to 8
- memory_values: bfloat16 [4096, 1024], P('sp', 'tp'), may hold values from -6 to 6
- input_gate_logits: float32 [8, 4096], P('tp', 'sp'), may hold values from -64 to 160
- forget_gate_logits: float32 [8, 4096], P('tp', 'sp'), may hold values from -0.1 to 20
- extra_log_decay: float32 [8, 4096], P('tp', 'sp'), may hold values from -1.4 to 0
- residual: bfloat16 [4096, 2048], P(('sp', 'tp')), may hold values from -6 to 6
- cell_output_weight: bfloat16 [1024, 2048], P('tp', 'sp'), may hold values from -0.1875 to 0.1875
- expert_norm_gain: float32 [2048], replicated, may hold values from 0.1 to 1.9
- expert_gate_weight: bfloat16 [8, 2048, 3584], P('sp', None, 'tp'), may hold values from -0.125 to 0.125
- expert_up_weight: bfloat16 [8, 2048, 3584], P('sp', None, 'tp'), may hold values from -0.125 to 0.125
- expert_down_weight: bfloat16 [8, 3584, 2048], P('sp', 'tp'), may hold values from -0.09375 to 0.09375
- routed_expert_index: int32 [4096, 2], P('sp'), may hold values from 0 to 7, as said below
- routed_expert_weight: float32 [4096, 2], P(('sp', 'tp')), may hold values from 0.1 to 1
Outputs:
- layer_out: bfloat16 [4096, 2048], P(('sp', 'tp'))
Inputs may be any that keep to these rules, and one draw needn't show every extreme that they name: `routed_expert_index`: each row names 2 different experts. In each aligned block of 128 rows (the rows of one device after the cell) no expert is named more than 40 times, and one expert is named exactly 40 times in every block.
All inputs are finite; a program needn't handle non-finite values.
Results may differ from a plain program's by a relative error of at most 0.013.
Values may be sent and summed in bfloat16 or wider, within the bound.
A program may use at most 128 MiB of HBM per device.

v0:
```python
import functools
import jax
import jax.numpy as jnp
from jax import lax
from jax.experimental import pallas as pl
from jax.experimental.pallas import tpu as pltpu
from jax.sharding import PartitionSpec as P

highest = lax.Precision.HIGHEST
lowest = -1e30
epsilon = 1e-06


def places():
    sp, tp = lax.axis_index("sp"), lax.axis_index("tp")
    n = lax.axis_size("sp")
    return sp, tp, n, tp + 1 - 2 * (tp % 2), (tp + 2) % 4


def greet(devices):
    barrier = pltpu.get_barrier_semaphore()
    for device in devices:
        pl.semaphore_signal(
            barrier, inc=1, device_id=device, device_id_type=pl.DeviceIdType.MESH
        )
    pl.semaphore_wait(barrier, len(devices))


def remote(src, dst, send, recv, device):
    return pltpu.make_async_remote_copy(
        src_ref=src,
        dst_ref=dst,
        send_sem=send,
        recv_sem=recv,
        device_id=device,
        device_id_type=pl.DeviceIdType.MESH,
    )


def far_first(n):
    return sorted(range(1, n), key=lambda k: abs(2 * k - n))


def dispatch_kernel(x_ref, out_ref, send_sems, recv_sems):
    sp, tp, n, p, q = places()
    peers = [((sp + k) % n, tp) for k in range(1, n)]
    greet(peers + [(sp, p), (sp, q)])
    across, first, late = {}, {}, []
    for k in far_first(n):
        copy = remote(
            x_ref.at[(sp + k) % n], out_ref.at[tp, sp],
            send_sems.at[0, k], recv_sems.at[0, k], peers[k - 1],
        )
        copy.start()
        first[k] = copy

    def relay(k):
        across[k].wait_recv()
        s = (sp - k + n) % n
        copy = remote(
            out_ref.at[q, s], out_ref.at[q, s], send_sems.at[3, k], recv_sems.at[3, k], (sp, p)
        )
        copy.start()
        late.append(copy)

    order = [0] + far_first(n)
    for step, k in enumerate(order):
        s = (sp - k + n) % n
        if k == 0:
            src = x_ref.at[sp]
        else:
            first[k].wait_recv()
            src = out_ref.at[tp, s]
        copy = remote(src, out_ref.at[tp, s], send_sems.at[1, k], recv_sems.at[1, k], (sp, q))
        copy.start()
        across[k] = copy
        copy = remote(src, out_ref.at[tp, s], send_sems.at[2, k], recv_sems.at[2, k], (sp, p))
        copy.start()
        late.append(copy)
        if k == 0:
            out_ref[tp, sp] = x_ref[sp]
        else:
            relay(order[step - 1])
    relay(order[-1])
    for copy in late:
        copy.wait()
    for copy in list(first.values()) + list(across.values()):
        copy.wait_send()


def dispatch(x):
    n, rows, width = x.shape
    return pl.pallas_call(
        dispatch_kernel,
        out_shape=jax.ShapeDtypeStruct((4, n, rows, width), x.dtype),
        in_specs=[pl.BlockSpec(memory_space=pltpu.VMEM)],
        out_specs=pl.BlockSpec(memory_space=pltpu.VMEM),
        scratch_shapes=[pltpu.SemaphoreType.DMA((4, n)), pltpu.SemaphoreType.DMA((4, n))],
        compiler_params=pltpu.CompilerParams(
            collective_id=1, has_side_effects=True, vmem_limit_bytes=58 * 2**20
        ),
    )(x)


def collect_kernel(back, x_ref, out_ref, near, sent, far, result, send_sems, recv_sems):
    sp, tp, n, p, q = places()
    chunks = x_ref.shape[1]
    offsets = far_first(n) + [0]
    peers = [((sp + k) % n, tp) for k in offsets[:-1]] if back else []
    greet(peers + [(sp, p), (sp, q)])

    def at(k):
        return (sp + offsets[k]) % n if back else k

    near_far, near_own, crossing, homeward = [], [], [], []
    for k in range(chunks):
        copy = remote(
            x_ref.at[(p + 2) % 4, at(k)], near.at[0, k],
            send_sems.at[0, k], recv_sems.at[0, k], (sp, p),
        )
        copy.start()
        near_far.append(copy)
    for k in range(chunks):
        copy = remote(
            x_ref.at[p, at(k)], near.at[1, k], send_sems.at[1, k], recv_sems.at[1, k], (sp, p)
        )
        copy.start()
        near_own.append(copy)
    for k in range(chunks):
        near_far[k].wait_recv()
        total = x_ref[q, at(k)].astype(jnp.float32) + near[0, k].astype(jnp.float32)
        sent[k] = total.astype(jnp.bfloat16)
        copy = remote(sent.at[k], far.at[k], send_sems.at[2, k], recv_sems.at[2, k], (sp, q))
        copy.start()
        crossing.append(copy)
    for k in range(chunks):
        near_own[k].wait_recv()
        crossing[k].wait_recv()
        total = x_ref[tp, at(k)].astype(jnp.float32) + near[1, k].astype(jnp.float32)
        total = (total + far[k].astype(jnp.float32)).astype(jnp.bfloat16)
        if not back:
            out_ref[k] = total
        elif k == chunks - 1:
            out_ref[sp] = total
        else:
            result[k] = total
            copy = remote(
                result.at[k], out_ref.at[sp], send_sems.at[3, k], recv_sems.at[3, k], peers[k]
            )
            copy.start()
            homeward.append(copy)
    for copy in homeward:
        copy.wait()
    for copy in near_far + near_own + crossing:
        copy.wait_send()


def collect(x, back):
    _, n, rows, width = x.shape
    block = (n, rows, width)
    return pl.pallas_call(
        functools.partial(collect_kernel, back),
        out_shape=jax.ShapeDtypeStruct(block, x.dtype),
        in_specs=[pl.BlockSpec(memory_space=pltpu.VMEM)],
        out_specs=pl.BlockSpec(memory_space=pltpu.VMEM),
        scratch_shapes=[
            pltpu.VMEM((2,) + block, x.dtype),
            pltpu.VMEM(block, x.dtype),
            pltpu.VMEM(block, x.dtype),
            pltpu.VMEM(block if back else (1, 16, 128), x.dtype),
            pltpu.SemaphoreType.DMA((4, n)),
            pltpu.SemaphoreType.DMA((4, n)),
        ],
        compiler_params=pltpu.CompilerParams(
            collective_id=2 if back else 3, has_side_effects=True, vmem_limit_bytes=58 * 2**20
        ),
    )(x)


def spread_kernel(x_ref, out_ref, send_sems, recv_sems):
    sp, tp, n, _, _ = places()
    half = n // 2
    twin = sp + 1 - 2 * (sp % 2)
    peers = [((sp + 2 * k) % n, tp) for k in range(1, half)]
    greet(peers + [(twin, tp)])
    first, second = [None], []
    for k in range(1, half):
        copy = remote(
            x_ref, out_ref.at[sp], send_sems.at[0, k], recv_sems.at[0, k], peers[k - 1]
        )
        copy.start()
        first.append(copy)
    for k in range(half):
        s = (sp - 2 * k + n) % n
        if k == 0:
            src = x_ref
        else:
            first[k].wait_recv()
            src = out_ref.at[s]
        copy = remote(src, out_ref.at[s], send_sems.at[1, k], recv_sems.at[1, k], (twin, tp))
        copy.start()
        second.append(copy)
        if k == 0:
            out_ref[sp] = x_ref[...]
    for copy in second:
        copy.wait()
    for copy in first[1:]:
        copy.wait_send()


def spread(x):
    n = lax.axis_size("sp")
    half = n // 2
    return pl.pallas_call(
        spread_kernel,
        out_shape=jax.ShapeDtypeStruct((n,) + x.shape, x.dtype),
        in_specs=[pl.BlockSpec(memory_space=pltpu.VMEM)],
        out_specs=pl.BlockSpec(memory_space=pltpu.VMEM),
        scratch_shapes=[pltpu.SemaphoreType.DMA((2, half)), pltpu.SemaphoreType.DMA((2, half))],
        compiler_params=pltpu.CompilerParams(
            collective_id=4, has_side_effects=True, vmem_limit_bytes=58 * 2**20
        ),
    )(x)


def carried_in(x):
    log_sum, mat, norm, top = x
    heads, dim, _ = mat.shape
    n, place = lax.axis_size("sp"), lax.axis_index("sp")
    scalars = jnp.broadcast_to(jnp.concatenate([log_sum, top])[:, None], (2 * heads, dim))
    packed = jnp.concatenate([mat.reshape(heads * dim, dim), norm, scalars], axis=0)
    used = packed.shape[0]
    packed = jnp.pad(packed, ((0, -used % 8), (0, 0)))
    everything = spread(packed)
    mats = everything[:, : heads * dim].reshape(n, heads, dim, dim)
    norms = everything[:, heads * dim : heads * dim + heads]
    logs = everything[:, heads * dim + heads : heads * dim + 2 * heads, 0]
    tops = everything[:, heads * dim + 2 * heads : heads * dim + 3 * heads, 0]
    index = jnp.arange(n)
    reached = index < place
    between = (index[None, :] > index[:, None]) & reached[None, :]
    decay = jnp.sum(jnp.where(between[:, :, None], logs[None], 0.0), axis=1)
    level = jnp.where(reached[:, None], tops + decay, lowest)
    prior_max = jnp.max(level, axis=0)
    scale = jnp.where(reached[:, None], jnp.exp(level - prior_max), 0.0)
    prior_mat = jnp.sum(scale[:, :, None, None] * mats, axis=0)
    prior_norm = jnp.sum(scale[:, :, None] * norms, axis=0)
    return prior_mat, prior_norm, prior_max


def block_pass(memory, inputs):
    state_mat, state_norm, state_max = memory
    queries, keys_blk, values_blk, gate_in, forget_log_value = inputs
    length = gate_in.shape[-1]
    running = jnp.cumsum(forget_log_value, axis=-1)
    causal = jnp.arange(length)[:, None] >= jnp.arange(length)[None, :]
    exponent = running[:, :, None] - running[:, None, :] + gate_in[:, None, :]
    exponent = jnp.where(causal[None], exponent, -jnp.inf)
    carried = running + state_max[:, None]
    row_max = jnp.maximum(carried, jnp.max(exponent, axis=-1))
    decays = jnp.exp(exponent - row_max[:, :, None])
    carry_scale = jnp.exp(carried - row_max)
    dispatch_affinity = jnp.einsum("htk,hsk->hts", queries, keys_blk, precision=highest) * decays
    numerator = carry_scale[:, :, None] * jnp.einsum(
        "hvk,htk->htv", state_mat, queries, precision=highest
    )
    numerator = numerator + jnp.einsum(
        "hts,hsv->htv", dispatch_affinity, values_blk, precision=highest
    )
    denominator = carry_scale * jnp.einsum(
        "hk,htk->ht", state_norm, queries, precision=highest
    ) + jnp.sum(dispatch_affinity, axis=-1)
    final_log = running[:, -1]
    log_prev = final_log + state_max
    log_keep = final_log[:, None] - running + gate_in
    new_max = jnp.maximum(log_prev, jnp.max(log_keep, axis=-1))
    prev_scale = jnp.exp(log_prev - new_max)
    retain = jnp.exp(log_keep - new_max[:, None])
    new_mat = prev_scale[:, None, None] * state_mat + jnp.einsum(
        "hsv,hsk->hvk", retain[:, :, None] * values_blk, keys_blk, precision=highest
    )
    new_norm = prev_scale[:, None] * state_norm + jnp.einsum(
        "hs,hsk->hk", retain, keys_blk, precision=highest
    )
    return ((new_mat, new_norm, new_max), (numerator, denominator, row_max))


def matrix_memory_step(
    memory_queries,
    memory_keys,
    memory_values,
    input_gate_logits,
    forget_gate_logits,
    extra_log_decay,
):
    tokens_here, channels = memory_queries.shape
    heads_here = input_gate_logits.shape[0]
    head_dim = channels // heads_here

    def heads_first(tensor):
        pieces = [
            tensor[:, head * head_dim : (head + 1) * head_dim] for head in range(heads_here)
        ]
        return jnp.stack(pieces).astype(jnp.float32)

    queries = heads_first(memory_queries) * head_dim ** (-0.5)
    forget_log_value = jax.nn.log_sigmoid(forget_gate_logits) + extra_log_decay
    block_size = min(tokens_here, 256)
    block_count = tokens_here // block_size

    def split_blocks(tensor):
        return jnp.moveaxis(
            tensor.reshape((heads_here, block_count, block_size) + tensor.shape[2:]), 1, 0
        )

    def join_blocks(tensor):
        return jnp.moveaxis(tensor, 0, 1).reshape((heads_here, tokens_here) + tensor.shape[3:])

    empty_state = (
        jnp.zeros((heads_here, head_dim, head_dim), jnp.float32),
        jnp.zeros((heads_here, head_dim), jnp.float32),
        jnp.full((heads_here,), lowest, jnp.float32),
    )
    members = (
        queries,
        heads_first(memory_keys),
        heads_first(memory_values),
        input_gate_logits,
        forget_log_value,
    )
    end_state, pieces = lax.scan(
        block_pass, empty_state, tuple((split_blocks(member) for member in members))
    )
    numerator, denominator, row_max = (join_blocks(member) for member in pieces)
    running = jnp.cumsum(forget_log_value, axis=-1)
    prior_mat, prior_norm, prior_max = carried_in((running[:, -1],) + tuple(end_state))
    reached = running + prior_max[:, None]
    joined = jnp.maximum(row_max, reached)
    local_scale = jnp.exp(row_max - joined)
    carry_scale = jnp.exp(reached - joined)
    numerator = local_scale[:, :, None] * numerator + carry_scale[:, :, None] * jnp.einsum(
        "hvk,htk->htv", prior_mat, queries, precision=highest
    )
    denominator = local_scale * denominator + carry_scale * jnp.einsum(
        "hk,htk->ht", prior_norm, queries, precision=highest
    )
    guarded = jnp.maximum(jnp.abs(denominator), jnp.exp(-joined))
    return ((numerator / guarded[:, :, None]).astype(jnp.bfloat16), heads_here, head_dim)


def slot_index(ids, experts, capacity):
    flat_ids = ids.reshape(-1)
    matches = (flat_ids[:, None] == jnp.arange(experts, dtype=jnp.int32)[None, :]).astype(jnp.int32)
    before = jnp.cumsum(matches, axis=0) - matches
    return flat_ids * capacity + jnp.sum(before * matches, axis=1)


def local(
    memory_queries,
    memory_keys,
    memory_values,
    input_gate_logits,
    forget_gate_logits,
    extra_log_decay,
    residual,
    cell_output_weight,
    expert_norm_gain,
    expert_gate_weight,
    expert_up_weight,
    expert_down_weight,
    routed_expert_index,
    routed_expert_weight,
):
    hidden, heads_here, head_dim = matrix_memory_step(
        memory_queries,
        memory_keys,
        memory_values,
        input_gate_logits,
        forget_gate_logits,
        extra_log_decay,
    )
    weight_piece = lax.all_gather(cell_output_weight, "sp", axis=1, tiled=True)
    shaped = weight_piece.reshape(heads_here, head_dim, weight_piece.shape[1])
    partial_rows = jnp.einsum(
        "htd,hdc->tc", hidden, shaped, preferred_element_type=jnp.float32
    ).astype(jnp.bfloat16)
    row_count, model_width = residual.shape
    projected = collect(partial_rows.reshape(4, 4, row_count // 4, model_width), False)
    projected = projected.reshape(row_count, model_width).astype(jnp.float32)
    mixed_rows = (residual.astype(jnp.float32) + projected).astype(jnp.bfloat16)
    mixed_wide = mixed_rows.astype(jnp.float32)
    norm_scale = lax.rsqrt(jnp.mean(mixed_wide * mixed_wide, axis=-1, keepdims=True) + epsilon)
    normed = (mixed_wide * norm_scale * expert_norm_gain).astype(jnp.bfloat16)
    sp_size = lax.axis_size("sp")
    top_count = routed_expert_index.shape[1]
    experts = sp_size * expert_gate_weight.shape[0]
    assigned = row_count * top_count
    capacity = max(2, assigned * 5 // (4 * experts))
    own_ids = lax.dynamic_slice_in_dim(
        routed_expert_index, lax.axis_index("tp") * row_count, row_count, 0
    )
    own_slots = slot_index(own_ids, experts, capacity)
    slots = own_slots.reshape(row_count, top_count)
    at_slot = slots[:, :, None] == jnp.arange(experts * capacity, dtype=jnp.int32)
    chosen = jnp.any(at_slot, axis=1).astype(jnp.bfloat16)
    outgoing = lax.dot_general(
        chosen, normed, (((0,), (0,)), ((), ())), preferred_element_type=jnp.float32
    ).astype(jnp.bfloat16)
    arrived = dispatch(outgoing.reshape(experts, capacity, model_width))
    flat_rows = arrived.reshape(-1, model_width)
    gate_pre = jnp.dot(flat_rows, expert_gate_weight[0], preferred_element_type=jnp.float32)
    up_pre = jnp.dot(flat_rows, expert_up_weight[0], preferred_element_type=jnp.float32)
    hidden_act = (jax.nn.silu(gate_pre) * up_pre).astype(jnp.bfloat16)
    group_term = jnp.dot(hidden_act, expert_down_weight[0], preferred_element_type=jnp.float32)
    group_term = lax.optimization_barrier(group_term.astype(jnp.bfloat16)).astype(jnp.float32)
    returned = collect(group_term.astype(jnp.bfloat16).reshape(arrived.shape), True)
    share = jnp.sum(jnp.where(at_slot, routed_expert_weight[:, :, None], 0.0), axis=1)
    routed_sum = jnp.dot(
        share,
        returned.reshape(experts * capacity, model_width).astype(jnp.float32),
        precision=highest,
    )
    return (mixed_wide + routed_sum).astype(jnp.bfloat16)


def solution(mesh):
    return jax.shard_map(
        local,
        mesh=mesh,
        in_specs=(
            P("sp", "tp"),
            P("sp", "tp"),
            P("sp", "tp"),
            P("tp", "sp"),
            P("tp", "sp"),
            P("tp", "sp"),
            P(("sp", "tp"), None),
            P("tp", "sp"),
            P(),
            P("sp", None, "tp"),
            P("sp", None, "tp"),
            P("sp", "tp", None),
            P("sp", None),
            P(("sp", "tp"), None),
        ),
        out_specs=P(("sp", "tp"), None),
        check_vma=False,
    )
```

profile of v0, /device:TPU:0, one launch (start us, length us, event | category | flops | bytes accessed | tf_op | source)
XLA Modules:
  0.0 221.2 jit_solution(4119506276037118616)
XLA Ops:
  6.5 0.7 all-gather.2.cloned.1.call-update
  7.7 1.0 slice_bitcast_fusion.1
  8.8 1.0 fusion.74
  9.8 1.0 fusion.73
  10.8 0.7 fusion.57
  11.7 11.3 %while.21 = (s32[]{:T(128)}, f32[2,128,128]{2,1,0:T(8,128)S(1)}, f32[2,128]{1,0:T(2,128)S(1)}, f32[2]{0:T(128)S(1)}, f32[2,2,256,128]{3,2,0,1:T(8,128)S(1)}, /*i...) while((s32[]{:T(128)}, f32[2,128,128]{2,1,0:T(8,128)S(1)}, ...), condition=%wide.region_6.7_spmd.clone, body=%wide.region_0.6_spmd.clone.sunk | while | flops 607329536 | bytes 4625314 | solution.py:331
  11.7 0.6 reduce-window.38
  13.5 0.6 fusion.130
  15.5 1.1 fusion.132
  16.6 0.7 convolution_add_fusion.4
  17.4 0.6 reduce-window.38
  19.1 0.6 fusion.130
  21.1 1.1 fusion.132
  22.3 0.7 convolution_add_fusion.4
  23.0 0.6 reduce-window.22
  24.4 0.7 pad.4.x_ref
  25.1 28.9 %shard_map.136 = f32[8,264,128]{2,1,0:T(8,128)} custom-call(f32[264,128]{1,0:T(8,128)} %pad.4.x_ref), custom_call_target="tpu_custom_call" | custom-call | tf_op jit(solution)/shard_map/pallas_call | solution.py:214
  54.0 0.8 fusion.72
  55.4 0.8 exponential_select_fusion
  56.4 0.6 reduce-window.26
  57.5 0.8 multiply_reduce_fusion.1
  58.7 1.6 multiply_reduce_fusion
  61.1 0.7 fusion.41
  61.8 3.4 %bitcast_convert_fusion = bf16[512,2048]{1,0:T(8,128)(2,1)} fusion(bf16[2,512,128]{2,1,0:T(8,128)(2,1)S(1)} %fusion.41, bf16[2,128,2048]{2,1,0:T(8,128)(2,1)} %bitcast.244), kind=kOutput, calls=%fused_computation.60 | convolution fusion | flops 537919488 | bytes 3407872 | tf_op jit(solution)/shard_map/htd,hdc->tc/dot_general | solution.py:384
  65.2 18.2 %shard_map.137 = bf16[4,32,2048]{2,1,0:T(8,128)(2,1)} custom-call(bf16[4,4,32,2048]{3,2,1,0:T(8,128)(2,1)} %bitcast.238), custom_call_target="tpu_custom_call" | custom-call | tf_op jit(solution)/shard_map/pallas_call | solution.py:161
  83.4 1.3 fusion.42
  84.8 1.7 convolution_convert_fusion.1
  86.5 54.6 %shard_map.138 = bf16[4,8,40,2048]{3,2,1,0:T(8,128)(2,1)} custom-call(bf16[8,40,2048]{2,1,0:T(8,128)(2,1)} %bitcast.243), custom_call_target="tpu_custom_call" | custom-call | tf_op jit(solution)/shard_map/pallas_call | solution.py:93
  141.1 8.9 %fusion.36 = f32[1280,896]{1,0:T(8,128)} fusion(bf16[1280,2048]{1,0:T(8,128)(2,1)} %bitcast.239, bf16[1,2048,896]{2,1,0:T(8,128)(2,1)S(1)} %copy-done.5), kind=kOutput, calls=%fused_computation.63 | convolution fusion | flops 4697620480 | bytes 13500416 | tf_op jit(solution)/shard_map/dot_general | solution.py:411
  150.0 17.6 %convolution_convert_fusion = bf16[1280,2048]{1,0:T(8,128)(2,1)} fusion(bf16[1,896,2048]{2,1,0:T(8,128)(2,1)} %param.27, f32[1280,896]{1,0:T(8,128)} %fusion.36, bf16[1280,2048]{1,0:T(8,128)(2,1)} %bitcast.240, bf16[1,2048,896]{2,1,0:T(8,128)(2,1)} %param.26), kind=kOutput, calls=%fused_computation.58 | convolution fusion | flops 9404743680 | bytes 22413312 | tf_op jit(solution)/shard_map/dot_general | solution.py:414
  167.6 43.6 %shard_map.139 = bf16[8,40,2048]{2,1,0:T(8,128)(2,1)} custom-call(bf16[4,8,40,2048]{3,2,1,0:T(8,128)(2,1)} %bitcast.241), custom_call_target="tpu_custom_call" | custom-call | tf_op jit(solution)/shard_map/pallas_call | solution.py:161
  211.2 3.2 %fusion.38 = bf16[128,2048]{1,0:T(8,128)(2,1)} fusion(f32[128,320]{0,1:T(8,128)S(1)} %select_reduce_fusion, bf16[320,2048]{1,0:T(8,128)(2,1)} %bitcast.242, bf16[128,2048]{1,0:T(8,128)(2,1)S(1)} %get-tuple-element.153), kind=kOutput, calls=%fused_computation.67 | convolution fusion | flops 1007419392 | bytes 2523136 | tf_op jit(solution)/shard_map/dot_general | solution.py:418
  (104 shorter events, 8.7 us)
Async XLA Ops:
  6.5 0.8 copy-start
  6.5 5.1 %copy-start.2 = (f32[2,512]{1,0:T(2,128)S(1)}, f32[2,512]{1,0:T(2,128)}, u32[]{:S(2)}) copy-start(f32[2,512]{1,0:T(2,128)} %param.19) | copy-start | bytes 12292
  6.5 55.3 %all-gather.2.cloned.1.call-start = ((), (), s32[]{:S(2)}) async-start(), calls=%async_computation | async-start | bytes 1179648 | tf_op jit(solution)/shard_map/all_gather | solution.py:382
  11.7 46.8 %copy-start.4 = (f32[128,2]{0,1:T(2,128)S(1)}, f32[128,2]{0,1:T(2,128)}, u32[]{:S(2)}) copy-start(f32[128,2]{0,1:T(2,128)} %param.29) | copy-start | bytes 3076
  61.8 21.7 %copy-start.1 = (bf16[128,2048]{1,0:T(8,128)(2,1)S(1)}, bf16[128,2048]{1,0:T(8,128)(2,1)}, u32[]{:S(2)}) copy-start(bf16[128,2048]{1,0:T(8,128)(2,1)} %param.22) | copy-start | bytes 1572868
  61.8 23.0 %copy-start.3 = (f32[2048]{0:T(1024)S(1)}, f32[2048]{0:T(1024)}, u32[]{:S(2)}) copy-start(f32[2048]{0:T(1024)} %param.24) | copy-start | bytes 24580
  86.5 54.6 %copy-start.5 = (bf16[1,2048,896]{2,1,0:T(8,128)(2,1)S(1)}, bf16[1,2048,896]{2,1,0:T(8,128)(2,1)}, u32[]{:S(2)}) copy-start(bf16[1,2048,896]{2,1,0:T(8,128)(2,1)} %param.25) | copy-start | bytes 11010052
Sparse Core Ops, SparseCore 0:
  9.4 45.7 all-gather.1
where the time goes:
time: 222 us; the launch traced here: 221 us
  Pallas kernels  145 us (65%)
  matrix products  42.7 us (19%)
  between operations  13.7 us (6%)
  other arithmetic  11.5 us (5%)
  local copies, waits for them, and re-layouts  7.03 us (3%)
    pallas_call x2, Pallas kernels, collect(): pl.pallas_call(functools.partial(collect_kernel, back), out_shape=jax.Sha...  61.8 us
    pallas_call x1, Pallas kernels, dispatch(): pl.pallas_call(dispatch_kernel, out_shape=jax.ShapeDtypeStruct((4, n, row...  54.6 us
    pallas_call x1, Pallas kernels, spread(): pl.pallas_call(spread_kernel, out_shape=jax.ShapeDtypeStruct((n,) + x.sha...  28.9 us
    dot_general x1, matrix products, local(): jnp.dot(hidden_act, expert_down_weight[0], preferred_element_type=jnp.flo...  17.6 us
    dot_general x1, matrix products, local(): jnp.dot(flat_rows, expert_gate_weight[0], preferred_element_type=jnp.floa...  8.91 us
  transfers between devices with their start and end apart: 1, of which 0 were waited for; matrix products, arithmetic and copies ran while one was open for 11% of the time, Pallas kernels for 13%

commit v1 on v0

--- a/solution.py
+++ b/solution.py
@@ -41,65 +41,201 @@
     return sorted(range(1, n), key=lambda k: abs(2 * k - n))
 
 
-def dispatch_kernel(x_ref, out_ref, send_sems, recv_sems):
+def flip(place, k, bits):
+    out = place
+    for b in range(bits):
+        step = 1 << b
+        out = out + ((k // step) % 2) * step * (1 - 2 * ((place // step) % 2))
+    return out
+
+
+def experts_kernel(
+    x_ref, gate_hbm, up_hbm, down_hbm, share_ref, mixed_ref, out_ref,
+    gate_up, down, arrive, part, near, sent, far, result, home,
+    weight_sems, direct_s, direct_r, across_s, across_r, side_s, side_r, relay_s, relay_r,
+    near_s, near_r, far_s, far_r, home_s, home_r,
+):
     sp, tp, n, p, q = places()
-    peers = [((sp + k) % n, tp) for k in range(1, n)]
-    greet(peers + [(sp, p), (sp, q)])
-    across, first, late = {}, {}, []
-    for k in far_first(n):
-        copy = remote(
-            x_ref.at[(sp + k) % n], out_ref.at[tp, sp],
-            send_sems.at[0, k], recv_sems.at[0, k], peers[k - 1],
-        )
-        copy.start()
-        first[k] = copy
-
-    def relay(k):
-        across[k].wait_recv()
-        s = (sp - k + n) % n
-        copy = remote(
-            out_ref.at[q, s], out_ref.at[q, s], send_sems.at[3, k], recv_sems.at[3, k], (sp, p)
-        )
-        copy.start()
-        late.append(copy)
-
-    order = [0] + far_first(n)
-    for step, k in enumerate(order):
-        s = (sp - k + n) % n
-        if k == 0:
-            src = x_ref.at[sp]
-        else:
-            first[k].wait_recv()
-            src = out_ref.at[tp, s]
-        copy = remote(src, out_ref.at[tp, s], send_sems.at[1, k], recv_sems.at[1, k], (sp, q))
-        copy.start()
-        across[k] = copy
-        copy = remote(src, out_ref.at[tp, s], send_sems.at[2, k], recv_sems.at[2, k], (sp, p))
-        copy.start()
-        late.append(copy)
-        if k == 0:
-            out_ref[tp, sp] = x_ref[sp]
-        else:
-            relay(order[step - 1])
-    relay(order[-1])
-    for copy in late:
-        copy.wait()
-    for copy in list(first.values()) + list(across.values()):
-        copy.wait_send()
-
-
-def dispatch(x):
+    bits = n.bit_length() - 1
+    half = n // 2
+    hidden = down.shape[0]
+    width = x_ref.shape[2]
+    rows = x_ref.shape[1]
+    pulls = [
+        pltpu.make_async_copy(gate_hbm.at[0], gate_up.at[:, pl.ds(0, hidden)], weight_sems.at[0]),
+        pltpu.make_async_copy(up_hbm.at[0], gate_up.at[:, pl.ds(hidden, hidden)], weight_sems.at[1]),
+        pltpu.make_async_copy(down_hbm.at[0], down, weight_sems.at[2]),
+    ]
+    for pull in pulls:
+        pull.start()
+    greet([(flip(sp, k, bits), tp) for k in range(1, n)] + [(sp, p), (sp, q)])
+
+    def turn(i):
+        late = i // half
+        return (1 - late) * (half + i) + late * (n - 1 - i)
+
+    def direct(i):
+        k = turn(i)
+        other = flip(sp, k, bits)
+        return remote(
+            x_ref.at[other], arrive.at[sp, tp], direct_s.at[i], direct_r.at[i], (other, tp)
+        )
+
+    def across(i, src):
+        s = flip(sp, turn(i), bits)
+        return remote(src(s), arrive.at[s, tp], across_s.at[i], across_r.at[i], (sp, q))
+
+    def side(i, src):
+        s = flip(sp, turn(i), bits)
+        return remote(src(s), arrive.at[s, tp], side_s.at[i], side_r.at[i], (sp, p))
+
+    def landed(s):
+        return arrive.at[s, tp]
+
+    def mine(s):
+        return x_ref.at[s]
+
+    def relay(i):
+        s = flip(sp, turn(i), bits)
+        return remote(
+            arrive.at[s, q], arrive.at[s, q], relay_s.at[i], relay_r.at[i], (sp, p)
+        )
+
+    def near_far(i):
+        s = flip(sp, turn(i), bits)
+        return remote(
+            part.at[s, (p + 2) % 4], near.at[0, i], near_s.at[0, i], near_r.at[0, i], (sp, p)
+        )
+
+    def near_own(i):
+        s = flip(sp, turn(i), bits)
+        return remote(part.at[s, p], near.at[1, i], near_s.at[1, i], near_r.at[1, i], (sp, p))
+
+    def crossing(i):
+        return remote(sent.at[i], far.at[i], far_s.at[i], far_r.at[i], (sp, q))
+
+    def homeward(i):
+        other = flip(sp, turn(i), bits)
+        return remote(result.at[i], home.at[sp], home_s.at[i], home_r.at[i], (other, tp))
+
+    @pl.loop(0, n - 1)
+    def _(i):
+        direct(i).start()
+
+    across(n - 1, mine).start()
+    side(n - 1, mine).start()
+    arrive[sp, tp] = x_ref[sp]
+    for pull in pulls:
+        pull.wait()
+
+    @pl.loop(0, n + 4)
+    def _(i):
+        @pl.when(i < n - 1)
+        def _():
+            direct(i).wait_recv()
+            across(i, landed).start()
+            side(i, landed).start()
+
+        @pl.when((i >= 1) & (i <= n))
+        def _():
+            across(i - 1, landed).wait_recv()
+            relay(i - 1).start()
+
+        @pl.when((i >= 2) & (i <= n + 1))
+        def _():
+            j = i - 2
+            s = flip(sp, turn(j), bits)
+            side(j, landed).wait_recv()
+            relay(j).wait_recv()
+            pre = jnp.dot(
+                arrive[s].reshape(4 * rows, width), gate_up[...],
+                preferred_element_type=jnp.float32,
+            )
+            gate = pre[:, :hidden]
+            act = (gate / (1.0 + jnp.exp(-gate)) * pre[:, hidden:]).astype(jnp.bfloat16)
+            out = jnp.dot(act, down[...], preferred_element_type=jnp.float32)
+            part[s] = out.astype(jnp.bfloat16).reshape(4, rows, width)
+            near_far(j).start()
+            near_own(j).start()
+
+        @pl.when((i >= 3) & (i <= n + 2))
+        def _():
+            j = i - 3
+            s = flip(sp, turn(j), bits)
+            near_far(j).wait_recv()
+            total = part[s, q].astype(jnp.float32) + near[0, j].astype(jnp.float32)
+            sent[j] = total.astype(jnp.bfloat16)
+            crossing(j).start()
+
+        @pl.when(i >= 4)
+        def _():
+            j = i - 4
+            s = flip(sp, turn(j), bits)
+            near_own(j).wait_recv()
+            crossing(j).wait_recv()
+            total = part[s, tp].astype(jnp.float32) + near[1, j].astype(jnp.float32)
+            result[j] = (total + far[j].astype(jnp.float32)).astype(jnp.bfloat16)
+
+            @pl.when(j < n - 1)
+            def _():
+                homeward(j).start()
+
+    home[sp] = result[n - 1]
+
+    @pl.loop(0, n - 1)
+    def _(i):
+        homeward(i).wait()
+        direct(i).wait_send()
+
+    @pl.loop(0, n)
+    def _(i):
+        across(i, landed).wait_send()
+        side(i, landed).wait_send()
+        relay(i).wait_send()
+        near_far(i).wait_send()
+        near_own(i).wait_send()
+        crossing(i).wait_send()
+
+    share = share_ref[...]
+    coarse = share.astype(jnp.bfloat16)
+    fine = (share - coarse.astype(jnp.float32)).astype(jnp.bfloat16)
+    back = home[...].reshape(n * rows, width)
+    routed = jnp.dot(coarse, back, preferred_element_type=jnp.float32)
+    routed = routed + jnp.dot(fine, back, preferred_element_type=jnp.float32)
+    out_ref[...] = (mixed_ref[...].astype(jnp.float32) + routed).astype(jnp.bfloat16)
+
+
+def experts_stage(x, gate, up, down, share, mixed):
     n, rows, width = x.shape
+    hidden = down.shape[1]
+    block = (n, rows, width)
+    vmem = pl.BlockSpec(memory_space=pltpu.VMEM)
+    hbm = pl.BlockSpec(memory_space=pl.ANY)
+    dma = pltpu.SemaphoreType.DMA
     return pl.pallas_call(
-        dispatch_kernel,
-        out_shape=jax.ShapeDtypeStruct((4, n, rows, width), x.dtype),
-        in_specs=[pl.BlockSpec(memory_space=pltpu.VMEM)],
-        out_specs=pl.BlockSpec(memory_space=pltpu.VMEM),
-        scratch_shapes=[pltpu.SemaphoreType.DMA((4, n)), pltpu.SemaphoreType.DMA((4, n))],
+        experts_kernel,
+        out_shape=jax.ShapeDtypeStruct(mixed.shape, mixed.dtype),
+        in_specs=[vmem, hbm, hbm, hbm, vmem, vmem],
+        out_specs=vmem,
+        scratch_shapes=[
+            pltpu.VMEM((width, 2 * hidden), x.dtype),
+            pltpu.VMEM((hidden, width), x.dtype),
+            pltpu.VMEM((n, 4, rows, width), x.dtype),
+            pltpu.VMEM((n, 4, rows, width), x.dtype),
+            pltpu.VMEM((2,) + block, x.dtype),
+            pltpu.VMEM(block, x.dtype),
+            pltpu.VMEM(block, x.dtype),
+            pltpu.VMEM(block, x.dtype),
+            pltpu.VMEM(block, x.dtype),
+            dma((3,)),
+        ]
+        + [dma((n,))] * 8
+        + [dma((2, n))] * 2
+        + [dma((n,))] * 4,
         compiler_params=pltpu.CompilerParams(
-            collective_id=1, has_side_effects=True, vmem_limit_bytes=58 * 2**20
+            collective_id=1, has_side_effects=True, vmem_limit_bytes=60 * 2**20
         ),
-    )(x)
+    )(x, gate, up, down, share, mixed)
 
 
 def collect_kernel(back, x_ref, out_ref, near, sent, far, result, send_sems, recv_sems):
@@ -406,21 +542,22 @@
     outgoing = lax.dot_general(
         chosen, normed, (((0,), (0,)), ((), ())), preferred_element_type=jnp.float32
     ).astype(jnp.bfloat16)
-    arrived = dispatch(outgoing.reshape(experts, capacity, model_width))
-    flat_rows = arrived.reshape(-1, model_width)
-    gate_pre = jnp.dot(flat_rows, expert_gate_weight[0], preferred_element_type=jnp.float32)
-    up_pre = jnp.dot(flat_rows, expert_up_weight[0], preferred_element_type=jnp.float32)
-    hidden_act = (jax.nn.silu(gate_pre) * up_pre).astype(jnp.bfloat16)
-    group_term = jnp.dot(hidden_act, expert_down_weight[0], preferred_element_type=jnp.float32)
-    group_term = lax.optimization_barrier(group_term.astype(jnp.bfloat16)).astype(jnp.float32)
-    returned = collect(group_term.astype(jnp.bfloat16).reshape(arrived.shape), True)
+    padded = -(-capacity // 8) * 8
+    outgoing = jnp.pad(
+        outgoing.reshape(experts, capacity, model_width), ((0, 0), (0, padded - capacity), (0, 0))
+    )
     share = jnp.sum(jnp.where(at_slot, routed_expert_weight[:, :, None], 0.0), axis=1)
-    routed_sum = jnp.dot(
-        share,
-        returned.reshape(experts * capacity, model_width).astype(jnp.float32),
-        precision=highest,
-    )
-    return (mixed_wide + routed_sum).astype(jnp.bfloat16)
+    share = jnp.pad(
+        share.reshape(row_count, experts, capacity), ((0, 0), (0, 0), (0, padded - capacity))
+    )
+    return experts_stage(
+        outgoing,
+        expert_gate_weight,
+        expert_up_weight,
+        expert_down_weight,
+        share.reshape(row_count, experts * padded),
+        mixed_rows,
+    )
 
 
 def solution(mesh):

time: 222 us -> 185 us (0.83)
  matrix products: 42.7 us -> 13 us
  Pallas kernels: 145 us -> 136 us
  local copies, waits for them, and re-layouts: 7.03 us -> 9.74 us
    pallas_call x2 -> x1, Pallas kernels: 61.8 us -> 18.3 us  [collect(): pl.pallas_call(functools.partial(collect_kernel, back), out_shape=jax.Sha...]
    pallas_call x1, Pallas kernels: 54.6 us -> 86.7 us  [experts_stage(): pl.pallas_call(experts_kernel, out_shape=jax.ShapeDtypeStruct(mixed.shape...]
    dot_general x3 -> x0, matrix products: 29.6 us -> none  [the longest x1 17.6 us: local(): jnp.dot(hidden_act, expert_down_weight[0], preferred_element_type=jnp.flo...]
  transfers between devices with their start and end apart: 1 -> 1, of which waited for: 0 -> 0; matrix products, arithmetic and copies ran while one was open for 11% -> 14% of each run, Pallas kernels for 13% -> 17%
where the time goes in v1:
time: 185 us; the launch traced here: 184 us
  Pallas kernels  136 us (74%)
  between operations  13.7 us (7%)
  matrix products  13 us (7%)
  other arithmetic  10.8 us (6%)
  local copies, waits for them, and re-layouts  9.74 us (5%)
    pallas_call x1, Pallas kernels, experts_stage(): pl.pallas_call(experts_kernel, out_shape=jax.ShapeDtypeStruct(mixed.shape...  86.7 us
    pallas_call x1, Pallas kernels, spread(): pl.pallas_call(spread_kernel, out_shape=jax.ShapeDtypeStruct((n,) + x.sha...  31.1 us
    pallas_call x1, Pallas kernels, collect(): pl.pallas_call(functools.partial(collect_kernel, back), out_shape=jax.Sha...  18.3 us
  transfers between devices with their start and end apart: 1, of which 0 were waited for; matrix products, arithmetic and copies ran while one was open for 14% of the time, Pallas kernels for 17%

profile of v1, /device:TPU:0, one launch (start us, length us, event | category | flops | bytes accessed | tf_op | source)
XLA Modules:
  0.0 184.2 jit_solution(17148538378116718859)
XLA Ops:
  6.5 0.7 all-gather.2.cloned.1.call-update
  7.8 1.0 slice_bitcast_fusion.1
  8.8 1.0 fusion.68
  9.8 1.0 fusion.69
  11.0 11.3 %while.21 = (s32[]{:T(128)}, f32[2,128,128]{2,1,0:T(8,128)S(1)}, f32[2,128]{1,0:T(2,128)S(1)}, f32[2]{0:T(128)S(1)}, f32[2,2,256,128]{3,2,0,1:T(8,128)S(1)}, /*i...) while((s32[]{:T(128)}, f32[2,128,128]{2,1,0:T(8,128)S(1)}, ...), condition=%wide.region_10.11_spmd.clone, body=%wide.region_4.10_spmd.clone.sunk | while | flops 607329536 | bytes 4625314 | solution.py:467
  11.0 0.6 reduce-window.38
  12.8 0.6 fusion.112
  14.4 0.4 convolution_multiply_fusion.4
  14.8 1.1 fusion.114
  15.9 0.7 convolution_add_fusion.3
  16.7 0.6 reduce-window.38
  18.5 0.6 fusion.112
  20.1 0.4 convolution_multiply_fusion.4
  20.4 1.1 fusion.114
  21.6 0.7 convolution_add_fusion.3
  22.3 0.6 reduce-window.26
  23.8 0.7 pad.4.x_ref
  24.4 31.1 %shard_map.136 = f32[8,264,128]{2,1,0:T(8,128)} custom-call(f32[264,128]{1,0:T(8,128)} %pad.4.x_ref), custom_call_target="tpu_custom_call" | custom-call | tf_op jit(solution)/shard_map/pallas_call | solution.py:350
  55.5 0.8 fusion.67
  56.9 0.6 reduce-window.22
  58.0 0.9 exponential_select_fusion
  59.1 0.8 copy.51.share_ref
  59.9 0.8 multiply_reduce_fusion.1
  61.0 1.6 multiply_reduce_fusion
  62.5 0.5 fusion.44
  63.4 0.7 fusion.36
  64.1 3.3 %bitcast_convert_fusion = bf16[512,2048]{1,0:T(8,128)(2,1)} fusion(bf16[2,512,128]{2,1,0:T(8,128)(2,1)S(1)} %fusion.36, bf16[2,128,2048]{2,1,0:T(8,128)(2,1)} %bitcast.215), kind=kOutput, calls=%fused_computation.58 | convolution fusion | flops 537919488 | bytes 3407872 | tf_op jit(solution)/shard_map/htd,hdc->tc/dot_general | solution.py:520
  67.4 18.3 %shard_map.137 = bf16[4,32,2048]{2,1,0:T(8,128)(2,1)} custom-call(bf16[4,4,32,2048]{3,2,1,0:T(8,128)(2,1)} %bitcast.213), custom_call_target="tpu_custom_call" | custom-call | tf_op jit(solution)/shard_map/pallas_call | solution.py:297
  85.8 1.3 fusion.37
  87.1 1.6 convolution_convert_fusion
  88.7 86.7 %shard_map.138 = bf16[128,2048]{1,0:T(8,128)(2,1)} custom-call(bf16[8,40,2048]{2,1,0:T(8,128)(2,1)} %bitcast.214, bf16[1,2048,896]{2,1,0:T(8,128)(2,1)} %gate_hbm.1, bf16[1,2048,896]{2,1,0:T(8,128)(2,1)} %up_hbm.1, bf16[1,896,2048]{2,1,0:T(8,128)(2,1)} %down_hbm.1, f32[128,320]{1,0:T(8,128)} %copy.51.share_ref, bf16[128,2048]{1,0:T(8,128)(2,1)} %copy-done.1), custom_call_target="tpu_custom_call" | custom-call | tf_op jit(solution)/shard_map/pallas_call | solution.py:215
  175.5 1.9 %copy.137 = bf16[128,2048]{1,0:T(8,128)(2,1)} copy(bf16[128,2048]{1,0:T(8,128)(2,1)} %shard_map.138) | data formatting | bytes 1048576
  (106 shorter events, 7.5 us)
Async XLA Ops:
  6.5 0.8 copy-start
  6.5 4.3 %copy-start.6 = (f32[2,512]{1,0:T(2,128)S(1)}, f32[2,512]{1,0:T(2,128)}, u32[]{:S(2)}) copy-start(f32[2,512]{1,0:T(2,128)} %param.20) | copy-start | bytes 12292
  6.5 4.3 %copy-start.5 = (f32[2,512]{1,0:T(2,128)S(1)}, f32[2,512]{1,0:T(2,128)}, u32[]{:S(2)}) copy-start(f32[2,512]{1,0:T(2,128)} %param.21) | copy-start | bytes 12292
  6.5 57.6 %all-gather.2.cloned.1.call-start = ((), (), s32[]{:S(2)}) async-start(), calls=%async_computation | async-start | bytes 1179648 | tf_op jit(solution)/shard_map/all_gather | solution.py:518
  7.7 3.2 %copy-start.3 = (f32[2,512]{1,0:T(2,128)S(1)}, f32[2,512]{1,0:T(2,128)}, u32[]{:S(2)}) copy-start(f32[2,512]{1,0:T(2,128)} %param.19) | copy-start | bytes 12292
  22.3 36.6 %copy-start.7 = (f32[128,2]{0,1:T(2,128)S(1)}, f32[128,2]{0,1:T(2,128)}, u32[]{:S(2)}) copy-start(f32[128,2]{0,1:T(2,128)} %param.29) | copy-start | bytes 3076
  67.4 18.3 %copy-start.2 = (bf16[128,2048]{1,0:T(8,128)(2,1)S(1)}, bf16[128,2048]{1,0:T(8,128)(2,1)}, u32[]{:S(2)}) copy-start(bf16[128,2048]{1,0:T(8,128)(2,1)} %param.22) | copy-start | bytes 1572868
  67.4 19.7 %copy-start.4 = (f32[2048]{0:T(1024)S(1)}, f32[2048]{0:T(1024)}, u32[]{:S(2)}) copy-start(f32[2048]{0:T(1024)} %param.24) | copy-start | bytes 24580
  87.1 1.7 copy-start.1
Sparse Core Ops, SparseCore 0:
  9.4 48.8 all-gather.1

commit v2 on v1

v2 whole, which is shorter than its diff:
```python
import functools
import jax
import jax.numpy as jnp
from jax import lax
from jax.experimental import pallas as pl
from jax.experimental.pallas import tpu as pltpu
from jax.sharding import PartitionSpec as P

highest = lax.Precision.HIGHEST
lowest = -1e30
epsilon = 1e-06


def places():
    sp, tp = lax.axis_index("sp"), lax.axis_index("tp")
    n = lax.axis_size("sp")
    return sp, tp, n, tp + 1 - 2 * (tp % 2), (tp + 2) % 4


def greet(devices):
    barrier = pltpu.get_barrier_semaphore()
    for device in devices:
        pl.semaphore_signal(
            barrier, inc=1, device_id=device, device_id_type=pl.DeviceIdType.MESH
        )
    pl.semaphore_wait(barrier, len(devices))


def remote(src, dst, send, recv, device):
    return pltpu.make_async_remote_copy(
        src_ref=src,
        dst_ref=dst,
        send_sem=send,
        recv_sem=recv,
        device_id=device,
        device_id_type=pl.DeviceIdType.MESH,
    )


def flip(place, k, bits):
    out = place
    for b in range(bits):
        step = 1 << b
        out = out + ((k // step) % 2) * step * (1 - 2 * ((place // step) % 2))
    return out


def narrow(x):
    coarse = x.astype(jnp.bfloat16)
    return coarse, (x - coarse.astype(jnp.float32)).astype(jnp.bfloat16)


def matmul(a, b):
    return jnp.dot(a, b, preferred_element_type=jnp.float32)


def matmul_t(a, b):
    return lax.dot_general(a, b, (((0,), (0,)), ((), ())), preferred_element_type=jnp.float32)


def matmul_nt(a, b):
    return lax.dot_general(a, b, (((1,), (1,)), ((), ())), preferred_element_type=jnp.float32)


def stack_rows(pieces, length):
    used = sum(piece.shape[0] for piece in pieces)
    return jnp.concatenate(list(pieces) + [jnp.zeros((-used % 8, length), jnp.float32)], axis=0)


def running_sum(x):
    rows, length = x.shape
    parts, rest = [], x
    for _ in range(3):
        part = rest.astype(jnp.bfloat16).astype(jnp.float32)
        parts.append(part)
        rest = rest - part
    stacked = stack_rows(parts, length).astype(jnp.bfloat16)
    at = lax.broadcasted_iota(jnp.int32, (length, length), 0)
    to = lax.broadcasted_iota(jnp.int32, (length, length), 1)
    sums = matmul(stacked, jnp.where(at <= to, 1.0, 0.0).astype(jnp.bfloat16))
    return sums[:rows] + sums[rows : 2 * rows] + sums[2 * rows : 3 * rows]


def running_max(x):
    length = x.shape[1]
    lane = lax.broadcasted_iota(jnp.int32, x.shape, 1)
    step = 1
    while step < length:
        x = jnp.maximum(x, jnp.where(lane >= step, pltpu.roll(x, step, 1), lowest))
        step *= 2
    return x


def slot_tables(ids, weights, experts, capacity, padded):
    rows = ids.shape[1]
    names = lax.broadcasted_iota(jnp.int32, (experts, rows), 0)
    hits = [ids[j : j + 1] == names for j in range(ids.shape[0])]
    named = sum(jnp.where(hit, 1.0, 0.0) for hit in hits)
    at = lax.broadcasted_iota(jnp.int32, (rows, rows), 0)
    to = lax.broadcasted_iota(jnp.int32, (rows, rows), 1)
    before = matmul(named.astype(jnp.bfloat16), jnp.where(at < to, 1.0, 0.0).astype(jnp.bfloat16))
    slot = lax.broadcasted_iota(jnp.int32, (experts * padded, rows), 0)
    chosen, share = 0.0, 0.0
    for j, hit in enumerate(hits):
        rank = jnp.sum(jnp.where(hit, before, 0.0), axis=0, keepdims=True)
        here = (ids[j : j + 1] * padded + rank.astype(jnp.int32)) == slot
        chosen = chosen + jnp.where(here, 1.0, 0.0)
        share = share + jnp.where(here, weights[j : j + 1], 0.0)
    return chosen.astype(jnp.bfloat16), share


def cell_kernel(
    experts, capacity, padded,
    q_ref, k_ref, v_ref, in_ref, forget_ref, extra_ref, res_ref, w_ref, gain_ref, ids_ref, wts_ref,
    out_ref, mixed_ref, share_ref,
    mine, mats, tiny_mine, tiny, pieces, pairs, hid, partial, near, sent, far,
    mat_s, mat_r, tiny_s, tiny_r, piece_s, piece_r, near_s, near_r, far_s, far_r,
):
    sp, tp, n, p, q = places()
    bits = n.bit_length() - 1
    length, channels = q_ref.shape
    heads = in_ref.shape[0]
    dim = channels // heads
    rows, width = res_ref.shape
    columns = w_ref.shape[1]
    evens = list(range(n - 2, 0, -2))
    evens = evens[len(evens) // 2 :][:1] + evens[: len(evens) // 2] + evens[len(evens) // 2 + 1 :]

    def at(k):
        return flip(sp, k, bits)

    def mat_copy(k):
        src = mine if k < 2 else (mine if k % 2 == 0 else mats.at[at(k - 1)])
        slot = sp if k % 2 == 0 or k == 1 else at(k - 1)
        to = at(1) if k % 2 else at(k)
        return remote(src, mats.at[slot], mat_s.at[k], mat_r.at[k], (to, tp))

    def tiny_copy(k):
        src = tiny_mine if k % 2 == 0 or k == 1 else tiny.at[at(k - 1)]
        slot = sp if k % 2 == 0 or k == 1 else at(k - 1)
        to = at(1) if k % 2 else at(k)
        return remote(src, tiny.at[slot], tiny_s.at[k], tiny_r.at[k], (to, tp))

    def piece_copy(k):
        src = w_ref if k % 2 == 0 or k == 1 else pieces.at[at(k - 1)]
        slot = sp if k % 2 == 0 or k == 1 else at(k - 1)
        to = at(1) if k % 2 else at(k)
        return remote(src, pieces.at[slot], piece_s.at[k], piece_r.at[k], (to, tp))

    greet([(at(k), tp) for k in [1] + evens] + [(sp, p), (sp, q)])
    piece_copy(1).start()
    piece_copy(evens[0]).start()

    logits = forget_ref[...]
    log_forget = (
        jnp.minimum(logits, 0.0) - jnp.log1p(jnp.exp(-jnp.abs(logits))) + extra_ref[...]
    )
    total = running_sum(log_forget)
    level = in_ref[...] - total
    peak = jnp.max(level, axis=1, keepdims=True)
    retain = jnp.exp(level - peak)
    retain_columns = jnp.transpose(stack_rows([retain], length))
    for h in range(heads):
        lanes = slice(h * dim, (h + 1) * dim)
        kept = narrow(v_ref[:, lanes].astype(jnp.float32) * retain_columns[:, h : h + 1])
        mat = matmul_t(k_ref[:, lanes], kept[0]) + matmul_t(k_ref[:, lanes], kept[1])
        mine[lanes, :] = mat.astype(jnp.bfloat16)
    coarse, fine = narrow(retain)
    sums = matmul(
        stack_rows([coarse.astype(jnp.float32), fine.astype(jnp.float32)], length).astype(jnp.bfloat16),
        k_ref[...],
    )
    norms = [
        sums[h : h + 1, h * dim : (h + 1) * dim]
        + sums[heads + h : heads + h + 1, h * dim : (h + 1) * dim]
        for h in range(heads)
    ]
    last = total[:, length - 1 : length]
    tiny_mine[...] = stack_rows(
        norms + [jnp.broadcast_to(last, (heads, dim)), jnp.broadcast_to(last + peak, (heads, dim))], dim
    )
    for k in evens + [1]:
        tiny_copy(k).start()
        mat_copy(k).start()
    for k in evens[1:]:
        piece_copy(k).start()
    mats[sp] = mine[...]
    tiny[sp] = tiny_mine[...]
    pieces[sp] = w_ref[...]

    top = running_max(level)
    top_columns = jnp.transpose(stack_rows([top], length))
    block = min(length, 256)
    for h in range(heads):
        lanes = slice(h * dim, (h + 1) * dim)
        widened = jnp.concatenate(
            [v_ref[:, lanes], jnp.ones((length, dim), jnp.bfloat16)], axis=1
        )
        for first in range(0, length, block):
            end = first + block
            scores = matmul_nt(q_ref[first:end, lanes], k_ref[:end, lanes])
            gap = level[h : h + 1, :end] - top_columns[first:end, h : h + 1]
            t = lax.broadcasted_iota(jnp.int32, (block, end), 0) + first
            s = lax.broadcasted_iota(jnp.int32, (block, end), 1)
            scores = scores * jnp.exp(jnp.where(s <= t, gap, lowest))
            coarse, fine = narrow(scores)
            pairs[h, first:end] = matmul(coarse, widened[:end]) + matmul(fine, widened[:end])

    chosen, share = slot_tables(ids_ref[...], wts_ref[...], experts, capacity, padded)
    share_ref[...] = share

    for k in evens:
        tiny_copy(k).wait_recv()
        tiny_copy(k + 1).start()
        mat_copy(k).wait_recv()
        mat_copy(k + 1).start()
    piece_copy(evens[0]).wait_recv()
    piece_copy(evens[0] + 1).start()
    for k in [1] + [k + 1 for k in evens]:
        tiny_copy(k).wait_recv()
        mat_copy(k).wait_recv()

    decay = jnp.zeros((heads, dim), jnp.float32)
    levels, flags = [None] * n, [None] * n
    for s in reversed(range(n)):
        flags[s] = jnp.where(s < sp, 1.0, 0.0)
        levels[s] = flags[s] * (tiny[s, 2 * heads : 3 * heads] + decay) + (1.0 - flags[s]) * lowest
        decay = decay + flags[s] * tiny[s, heads : 2 * heads]
    prior_top = functools.reduce(jnp.maximum, levels)
    scales = [jnp.exp(levels[s] - prior_top) * flags[s] for s in range(n)]
    prior_norm = sum(scales[s] * tiny[s, :heads] for s in range(n))
    norm_columns = jnp.transpose(stack_rows([prior_norm], dim))
    reach = jnp.broadcast_to(prior_top[:, :1], (heads, length))
    joined = jnp.maximum(top, reach)
    factors = jnp.transpose(
        stack_rows(
            [
                jnp.exp(top - joined),
                jnp.exp(reach - joined),
                jnp.exp(-(total + joined)) * dim**0.5,
            ],
            length,
        )
    )
    for h in range(heads):
        lanes = slice(h * dim, (h + 1) * dim)
        prior = sum(
            scales[s][h : h + 1] * mats[s, lanes, :].astype(jnp.float32) for s in range(n)
        )
        prior = jnp.concatenate(
            [prior, jnp.broadcast_to(norm_columns[:, h : h + 1], (dim, dim))], axis=1
        )
        coarse, fine = narrow(prior)
        carried = matmul(q_ref[:, lanes], coarse) + matmul(q_ref[:, lanes], fine)
        both = pairs[h] * factors[:, h : h + 1]
        both = both + carried * factors[:, heads + h : heads + h + 1]
        guard = jnp.maximum(
            jnp.abs(both[:, dim:]), factors[:, 2 * heads + h : 2 * heads + h + 1]
        )
        hid[:, lanes] = (both[:, :dim] / guard).astype(jnp.bfloat16)

    group = max(1, 256 // columns)
    chunk = group * columns
    count = width // chunk

    def pass_on(k):
        piece_copy(k).wait_recv()
        piece_copy(k + 1).start()

    def near_far(i):
        return remote(
            partial.at[i, (p + 2) % 4], near.at[0, i], near_s.at[0, i], near_r.at[0, i], (sp, p)
        )

    def near_own(i):
        return remote(partial.at[i, p], near.at[1, i], near_s.at[1, i], near_r.at[1, i], (sp, p))

    def crossing(i):
        return remote(sent.at[i], far.at[i], far_s.at[i], far_r.at[i], (sp, q))

    def cross(i):
        near_far(i).wait_recv()
        both = partial[i, q].astype(jnp.float32) + near[0, i].astype(jnp.float32)
        sent[i] = both.astype(jnp.bfloat16)
        crossing(i).start()

    if group == 1:
        order = [0, 1, evens[0], evens[0] + 1] + evens[1:] + [k + 1 for k in evens[1:]]
        spots = [at(k) for k in order]
    else:
        order = spots = list(range(count))
        for k in evens[1:]:
            pass_on(k)
        for k in [1] + [k + 1 for k in evens]:
            piece_copy(k).wait_recv()
    for i, k in enumerate(order):
        if group > 1:
            piece = jnp.concatenate([pieces[i * group + j] for j in range(group)], axis=1)
        else:
            if k % 2:
                piece_copy(k).wait_recv()
            elif k in evens[1:]:
                pass_on(k)
            piece = pieces[spots[i]]
        made = matmul(hid[...], piece).astype(jnp.bfloat16)
        partial[i] = made.reshape(length // rows, rows, chunk)
        near_far(i).start()
        near_own(i).start()
        if i:
            cross(i - 1)
    cross(count - 1)

    squares = jnp.zeros((rows, 1), jnp.float32)
    for i in range(count):
        near_own(i).wait_recv()
        crossing(i).wait_recv()
        where = pl.ds(pl.multiple_of(spots[i] * chunk, chunk), chunk)
        both = partial[i, tp].astype(jnp.float32) + near[1, i].astype(jnp.float32)
        both = both + far[i].astype(jnp.float32)
        mixed = (res_ref[:, where].astype(jnp.float32) + both).astype(jnp.bfloat16)
        mixed_ref[:, where] = mixed
        wide = mixed.astype(jnp.float32)
        squares = squares + jnp.sum(wide * wide, axis=1, keepdims=True)
    scale = lax.rsqrt(squares / width + epsilon)
    span = min(width, 512)
    for first in range(0, width, span):
        wide = mixed_ref[:, first : first + span].astype(jnp.float32)
        normed = (wide * scale * gain_ref[:, first : first + span]).astype(jnp.bfloat16)
        picked = matmul(chosen, normed).astype(jnp.bfloat16)
        out_ref[:, :, first : first + span] = picked.reshape(experts, padded, span)

    for k in range(1, n):
        tiny_copy(k).wait_send()
        mat_copy(k).wait_send()
        piece_copy(k).wait_send()
    for i in range(count):
        near_far(i).wait_send()
        near_own(i).wait_send()
        crossing(i).wait_send()


def cell_stage(capacity, q, k, v, gate_in, forget, extra, residual, weight, gain, ids, wts):
    n = lax.axis_size("sp")
    length, channels = q.shape
    heads = gate_in.shape[0]
    dim = channels // heads
    rows, width = residual.shape
    columns = weight.shape[1]
    chunk = max(1, 256 // columns) * columns
    count = width // chunk
    padded = -(-capacity // 8) * 8
    vmem = pl.BlockSpec(memory_space=pltpu.VMEM)
    dma = pltpu.SemaphoreType.DMA
    kind = residual.dtype
    return pl.pallas_call(
        functools.partial(cell_kernel, n, capacity, padded),
        out_shape=(
            jax.ShapeDtypeStruct((n, padded, width), kind),
            jax.ShapeDtypeStruct((rows, width), kind),
            jax.ShapeDtypeStruct((n * padded, rows), jnp.float32),
        ),
        in_specs=[vmem] * 11,
        out_specs=(vmem,) * 3,
        scratch_shapes=[
            pltpu.VMEM((channels, dim), kind),
            pltpu.VMEM((n, channels, dim), kind),
            pltpu.VMEM((8, dim), jnp.float32),
            pltpu.VMEM((n, 8, dim), jnp.float32),
            pltpu.VMEM((n, channels, columns), kind),
            pltpu.VMEM((heads, length, 2 * dim), jnp.float32),
            pltpu.VMEM((length, channels), kind),
            pltpu.VMEM((count, length // rows, rows, chunk), kind),
            pltpu.VMEM((2, count, rows, chunk), kind),
            pltpu.VMEM((count, rows, chunk), kind),
            pltpu.VMEM((count, rows, chunk), kind),
        ]
        + [dma((n,))] * 6
        + [dma((2, count))] * 2
        + [dma((count,))] * 2,
        compiler_params=pltpu.CompilerParams(
            collective_id=2, has_side_effects=True, vmem_limit_bytes=58 * 2**20
        ),
    )(q, k, v, gate_in, forget, extra, residual, weight, gain, ids, wts)


def experts_kernel(
    x_ref, gate_hbm, up_hbm, down_hbm, share_ref, mixed_ref, out_ref,
    gate_up, down, arrive, part, near, sent, far, result, home,
    weight_sems, direct_s, direct_r, across_s, across_r, side_s, side_r, relay_s, relay_r,
    near_s, near_r, far_s, far_r, home_s, home_r,
):
    sp, tp, n, p, q = places()
    bits = n.bit_length() - 1
    half = n // 2
    hidden = down.shape[0]
    width = x_ref.shape[2]
    rows = x_ref.shape[1]
    pulls = [
        pltpu.make_async_copy(gate_hbm.at[0], gate_up.at[:, pl.ds(0, hidden)], weight_sems.at[0]),
        pltpu.make_async_copy(up_hbm.at[0], gate_up.at[:, pl.ds(hidden, hidden)], weight_sems.at[1]),
        pltpu.make_async_copy(down_hbm.at[0], down, weight_sems.at[2]),
    ]
    for pull in pulls:
        pull.start()
    greet([(flip(sp, k, bits), tp) for k in range(1, n)] + [(sp, p), (sp, q)])

    def turn(i):
        late = i // half
        return (1 - late) * (half + i) + late * (n - 1 - i)

    def direct(i):
        k = turn(i)
        other = flip(sp, k, bits)
        return remote(
            x_ref.at[other], arrive.at[sp, tp], direct_s.at[i], direct_r.at[i], (other, tp)
        )

    def across(i, src):
        s = flip(sp, turn(i), bits)
        return remote(src(s), arrive.at[s, tp], across_s.at[i], across_r.at[i], (sp, q))

    def side(i, src):
        s = flip(sp, turn(i), bits)
        return remote(src(s), arrive.at[s, tp], side_s.at[i], side_r.at[i], (sp, p))

    def landed(s):
        return arrive.at[s, tp]

    def mine(s):
        return x_ref.at[s]

    def relay(i):
        s = flip(sp, turn(i), bits)
        return remote(
            arrive.at[s, q], arrive.at[s, q], relay_s.at[i], relay_r.at[i], (sp, p)
        )

    def near_far(i):
        s = flip(sp, turn(i), bits)
        return remote(
            part.at[s, (p + 2) % 4], near.at[0, i], near_s.at[0, i], near_r.at[0, i], (sp, p)
        )

    def near_own(i):
        s = flip(sp, turn(i), bits)
        return remote(part.at[s, p], near.at[1, i], near_s.at[1, i], near_r.at[1, i], (sp, p))

    def crossing(i):
        return remote(sent.at[i], far.at[i], far_s.at[i], far_r.at[i], (sp, q))

    def homeward(i):
        other = flip(sp, turn(i), bits)
        return remote(result.at[i], home.at[sp], home_s.at[i], home_r.at[i], (other, tp))

    @pl.loop(0, n - 1)
    def _(i):
        direct(i).start()

    across(n - 1, mine).start()
    side(n - 1, mine).start()
    arrive[sp, tp] = x_ref[sp]
    for pull in pulls:
        pull.wait()

    @pl.loop(0, n + 4)
    def _(i):
        @pl.when(i < n - 1)
        def _():
            direct(i).wait_recv()
            across(i, landed).start()
            side(i, landed).start()

        @pl.when((i >= 1) & (i <= n))
        def _():
            across(i - 1, landed).wait_recv()
            relay(i - 1).start()

        @pl.when((i >= 2) & (i <= n + 1))
        def _():
            j = i - 2
            s = flip(sp, turn(j), bits)
            side(j, landed).wait_recv()
            relay(j).wait_recv()
            pre = jnp.dot(
                arrive[s].reshape(4 * rows, width), gate_up[...],
                preferred_element_type=jnp.float32,
            )
            gate = pre[:, :hidden]
            act = (gate / (1.0 + jnp.exp(-gate)) * pre[:, hidden:]).astype(jnp.bfloat16)
            out = jnp.dot(act, down[...], preferred_element_type=jnp.float32)
            part[s] = out.astype(jnp.bfloat16).reshape(4, rows, width)
            near_far(j).start()
            near_own(j).start()

        @pl.when((i >= 3) & (i <= n + 2))
        def _():
            j = i - 3
            s = flip(sp, turn(j), bits)
            near_far(j).wait_recv()
            total = part[s, q].astype(jnp.float32) + near[0, j].astype(jnp.float32)
            sent[j] = total.astype(jnp.bfloat16)
            crossing(j).start()

        @pl.when(i >= 4)
        def _():
            j = i - 4
            s = flip(sp, turn(j), bits)
            near_own(j).wait_recv()
            crossing(j).wait_recv()
            total = part[s, tp].astype(jnp.float32) + near[1, j].astype(jnp.float32)
            result[j] = (total + far[j].astype(jnp.float32)).astype(jnp.bfloat16)

            @pl.when(j < n - 1)
            def _():
                homeward(j).start()

    home[sp] = result[n - 1]

    @pl.loop(0, n - 1)
    def _(i):
        homeward(i).wait()
        direct(i).wait_send()

    @pl.loop(0, n)
    def _(i):
        across(i, landed).wait_send()
        side(i, landed).wait_send()
        relay(i).wait_send()
        near_far(i).wait_send()
        near_own(i).wait_send()
        crossing(i).wait_send()

    share = share_ref[...]
    coarse, fine = narrow(share)
    back = home[...].reshape(n * rows, width)
    routed = matmul_t(coarse, back) + matmul_t(fine, back)
    out_ref[...] = (mixed_ref[...].astype(jnp.float32) + routed).astype(jnp.bfloat16)


def experts_stage(x, gate, up, down, share, mixed):
    n, rows, width = x.shape
    hidden = down.shape[1]
    block = (n, rows, width)
    vmem = pl.BlockSpec(memory_space=pltpu.VMEM)
    hbm = pl.BlockSpec(memory_space=pl.ANY)
    dma = pltpu.SemaphoreType.DMA
    return pl.pallas_call(
        experts_kernel,
        out_shape=jax.ShapeDtypeStruct(mixed.shape, mixed.dtype),
        in_specs=[vmem, hbm, hbm, hbm, vmem, vmem],
        out_specs=vmem,
        scratch_shapes=[
            pltpu.VMEM((width, 2 * hidden), x.dtype),
            pltpu.VMEM((hidden, width), x.dtype),
            pltpu.VMEM((n, 4, rows, width), x.dtype),
            pltpu.VMEM((n, 4, rows, width), x.dtype),
            pltpu.VMEM((2,) + block, x.dtype),
            pltpu.VMEM(block, x.dtype),
            pltpu.VMEM(block, x.dtype),
            pltpu.VMEM(block, x.dtype),
            pltpu.VMEM(block, x.dtype),
            dma((3,)),
        ]
        + [dma((n,))] * 8
        + [dma((2, n))] * 2
        + [dma((n,))] * 4,
        compiler_params=pltpu.CompilerParams(
            collective_id=1, has_side_effects=True, vmem_limit_bytes=60 * 2**20
        ),
    )(x, gate, up, down, share, mixed)


def local(
    memory_queries,
    memory_keys,
    memory_values,
    input_gate_logits,
    forget_gate_logits,
    extra_log_decay,
    residual,
    cell_output_weight,
    expert_norm_gain,
    expert_gate_weight,
    expert_up_weight,
    expert_down_weight,
    routed_expert_index,
    routed_expert_weight,
):
    row_count = residual.shape[0]
    experts = lax.axis_size("sp") * expert_gate_weight.shape[0]
    assigned = row_count * routed_expert_index.shape[1]
    capacity = max(2, assigned * 5 // (4 * experts))
    own_ids = lax.dynamic_slice_in_dim(
        routed_expert_index, lax.axis_index("tp") * row_count, row_count, 0
    )
    outgoing, mixed, share = cell_stage(
        capacity,
        memory_queries,
        memory_keys,
        memory_values,
        input_gate_logits,
        forget_gate_logits,
        extra_log_decay,
        residual,
        cell_output_weight,
        expert_norm_gain[None, :],
        own_ids.T,
        routed_expert_weight.T,
    )
    return experts_stage(
        outgoing, expert_gate_weight, expert_up_weight, expert_down_weight, share, mixed
    )


def solution(mesh):
    return jax.shard_map(
        local,
        mesh=mesh,
        in_specs=(
            P("sp", "tp"),
            P("sp", "tp"),
            P("sp", "tp"),
            P("tp", "sp"),
            P("tp", "sp"),
            P("tp", "sp"),
            P(("sp", "tp"), None),
            P("tp", "sp"),
            P(),
            P("sp", None, "tp"),
            P("sp", None, "tp"),
            P("sp", "tp", None),
            P("sp", None),
            P(("sp", "tp"), None),
        ),
        out_specs=P(("sp", "tp"), None),
        check_vma=False,
    )
```

time: 185 us -> 136 us (0.74)
  between operations: 13.7 us -> 0.02 us
  matrix products: 13 us -> 0 us
  other arithmetic: 10.8 us -> 0 us
  local copies, waits for them, and re-layouts: 9.74 us -> 3.13 us
  Pallas kernels: 136 us -> 132 us
    dot_general x16 -> x0, matrix products: 13 us -> none  [the longest x1 3.31 us: local(): jnp.einsum('htd,hdc->tc', hidden, shaped, preferred_element_type=jnp.floa...]
    reduce_sum x6 -> x0, other arithmetic: 3.95 us -> none  [the longest x1 1.58 us: carried_in(): prior_mat = jnp.sum(scale[:, :, None, None] * mats, axis=0)]
    slice x10 -> x0, local copies, waits for them, and re-layouts: 3.77 us -> none  [the longest x2 1.98 us: heads_first(): tensor[:, head * head_dim:(head + 1) * head_dim]]
    another operation x12 -> x0, other arithmetic: 3.16 us -> none
    pallas_call x2 -> x1, Pallas kernels: 49.4 us -> 46.5 us  [cell_stage(): pl.pallas_call(functools.partial(cell_kernel, n, capacity, padded), out_s...]
  transfers between devices with their start and end apart: 1 -> 0, of which waited for: 0 -> 0; matrix products, arithmetic and copies ran while one was open for 14% -> 0% of each run, Pallas kernels for 17% -> 0%
where the time goes in v2:
time: 136 us; the launch traced here: 135 us
  Pallas kernels  132 us (97%)
  local copies, waits for them, and re-layouts  3.13 us (2%)
    pallas_call x1, Pallas kernels, experts_stage(): pl.pallas_call(experts_kernel, out_shape=jax.ShapeDtypeStruct(mixed.shape...  85.7 us
    pallas_call x1, Pallas kernels, cell_stage(): pl.pallas_call(functools.partial(cell_kernel, n, capacity, padded), out_s...  46.5 us

profile of v2, /device:TPU:0, one launch (start us, length us, event | category | flops | bytes accessed | tf_op | source)
XLA Modules:
  0.0 135.3 jit_solution(17138218081136331701)
XLA Ops:
  0.0 0.0 copy-start
  0.0 0.7 copy-done
  0.7 0.6 dynamic-slice_bitcast_fusion.ids_ref
  1.3 46.5 %shard_map.136 = (bf16[8,40,2048]{2,1,0:T(8,128)(2,1)}, bf16[128,2048]{1,0:T(8,128)(2,1)}, f32[320,128]{1,0:T(8,128)}) custom-call(bf16[512,256]{1,0:T(8,128)(2,1)} %q_ref.1, bf16[512,256]{1,0:T(8,128)(2,1)} %k_ref.1, bf16[512,256]{1,0:T(8,128)(2,1)} %v_ref.1, f32[2,512]{1,0:T(2,128)} %in_ref.1, f32[2,512]{1,0:T(2,128)} %forget_ref.1, f32[2,512]{1,0:T(2,128)} %extra_ref.1, ...), custom_call_target="tpu_custom_call" | custom-call | tf_op jit(solution)/shard_map/pallas_call | solution.py:355
  47.8 85.7 %shard_map.137 = bf16[128,2048]{1,0:T(8,128)(2,1)} custom-call(bf16[8,40,2048]{2,1,0:T(8,128)(2,1)} %get-tuple-element.8.x_ref, bf16[1,2048,896]{2,1,0:T(8,128)(2,1)} %gate_hbm.1, bf16[1,2048,896]{2,1,0:T(8,128)(2,1)} %up_hbm.1, bf16[1,896,2048]{2,1,0:T(8,128)(2,1)} %down_hbm.1, f32[320,128]{1,0:T(8,128)} %get-tuple-element.9.share_ref, ...), custom_call_target="tpu_custom_call" | custom-call | tf_op jit(solution)/shard_map/pallas_call | solution.py:547
  133.4 1.9 %copy.16 = bf16[128,2048]{1,0:T(8,128)(2,1)} copy(bf16[128,2048]{1,0:T(8,128)(2,1)} %shard_map.137) | data formatting | bytes 1048576
Async XLA Ops:
  0.0 0.7 copy-start

commit v3 on v2

--- a/solution.py
+++ b/solution.py
@@ -17,13 +17,13 @@
     return sp, tp, n, tp + 1 - 2 * (tp % 2), (tp + 2) % 4
 
 
-def greet(devices):
+def announce(devices):
     barrier = pltpu.get_barrier_semaphore()
     for device in devices:
         pl.semaphore_signal(
             barrier, inc=1, device_id=device, device_id_type=pl.DeviceIdType.MESH
         )
-    pl.semaphore_wait(barrier, len(devices))
+    return len(devices)
 
 
 def remote(src, dst, send, recv, device):
@@ -109,22 +109,38 @@
     return chosen.astype(jnp.bfloat16), share
 
 
-def cell_kernel(
-    experts, capacity, padded,
-    q_ref, k_ref, v_ref, in_ref, forget_ref, extra_ref, res_ref, w_ref, gain_ref, ids_ref, wts_ref,
-    out_ref, mixed_ref, share_ref,
-    mine, mats, tiny_mine, tiny, pieces, pairs, hid, partial, near, sent, far,
-    mat_s, mat_r, tiny_s, tiny_r, piece_s, piece_r, near_s, near_r, far_s, far_r,
+def layer_kernel(
+    capacity, padded,
+    q_hbm, k_ref, v_ref, in_ref, forget_ref, extra_ref, res_hbm, w_hbm, gain_ref, ids_ref, wts_ref,
+    gate_hbm, up_hbm, down_hbm, out_ref,
+    q_ref, res_ref, mine, mats, tiny_mine, tiny, pieces, pairs, hid, partial, near, sent, far,
+    x_ref, mixed_ref, share_ref, gate_up, down, arrive, part, close, paid, other_half, result,
+    home, routed,
+    load_sems, mat_s, mat_r, tiny_s, tiny_r, piece_s, piece_r, near_s, near_r, far_s, far_r,
+    direct_s, direct_r, across_s, across_r, side_s, side_r, relay_s, relay_r,
+    close_s, close_r, paid_s, paid_r, home_s, home_r,
 ):
     sp, tp, n, p, q = places()
     bits = n.bit_length() - 1
-    length, channels = q_ref.shape
+    length, channels = k_ref.shape
     heads = in_ref.shape[0]
     dim = channels // heads
-    rows, width = res_ref.shape
-    columns = w_ref.shape[1]
-    evens = list(range(n - 2, 0, -2))
-    evens = evens[len(evens) // 2 :][:1] + evens[: len(evens) // 2] + evens[len(evens) // 2 + 1 :]
+    rows, width = out_ref.shape
+    columns = pieces.shape[2]
+    hidden = down.shape[0]
+    experts = n
+    count_greeted = announce([(flip(sp, k, bits), tp) for k in range(1, n)] + [(sp, p), (sp, q)])
+    loads = [
+        pltpu.make_async_copy(w_hbm, pieces.at[sp], load_sems.at[0]),
+        pltpu.make_async_copy(q_hbm, q_ref, load_sems.at[1]),
+        pltpu.make_async_copy(res_hbm, res_ref, load_sems.at[2]),
+        pltpu.make_async_copy(gate_hbm.at[0], gate_up.at[:, pl.ds(0, hidden)], load_sems.at[3]),
+        pltpu.make_async_copy(up_hbm.at[0], gate_up.at[:, pl.ds(hidden, hidden)], load_sems.at[4]),
+        pltpu.make_async_copy(down_hbm.at[0], down, load_sems.at[5]),
+    ]
+    for load in loads:
+        load.start()
+    evens = list(range(2, n, 2))
 
     def at(k):
         return flip(sp, k, bits)
@@ -142,14 +158,10 @@
         return remote(src, tiny.at[slot], tiny_s.at[k], tiny_r.at[k], (to, tp))
 
     def piece_copy(k):
-        src = w_ref if k % 2 == 0 or k == 1 else pieces.at[at(k - 1)]
         slot = sp if k % 2 == 0 or k == 1 else at(k - 1)
+        src = pieces.at[slot]
         to = at(1) if k % 2 else at(k)
         return remote(src, pieces.at[slot], piece_s.at[k], piece_r.at[k], (to, tp))
-
-    greet([(at(k), tp) for k in [1] + evens] + [(sp, p), (sp, q)])
-    piece_copy(1).start()
-    piece_copy(evens[0]).start()
 
     logits = forget_ref[...]
     log_forget = (
@@ -179,14 +191,16 @@
     tiny_mine[...] = stack_rows(
         norms + [jnp.broadcast_to(last, (heads, dim)), jnp.broadcast_to(last + peak, (heads, dim))], dim
     )
+    pl.semaphore_wait(pltpu.get_barrier_semaphore(), count_greeted)
     for k in evens + [1]:
         tiny_copy(k).start()
         mat_copy(k).start()
-    for k in evens[1:]:
+    loads[0].wait()
+    for k in [1] + evens:
         piece_copy(k).start()
     mats[sp] = mine[...]
     tiny[sp] = tiny_mine[...]
-    pieces[sp] = w_ref[...]
+    loads[1].wait()
 
     top = running_max(level)
     top_columns = jnp.transpose(stack_rows([top], length))
@@ -207,15 +221,14 @@
             pairs[h, first:end] = matmul(coarse, widened[:end]) + matmul(fine, widened[:end])
 
     chosen, share = slot_tables(ids_ref[...], wts_ref[...], experts, capacity, padded)
-    share_ref[...] = share
+    share_ref[...] = share.reshape(experts, padded, rows)
+    loads[2].wait()
 
     for k in evens:
         tiny_copy(k).wait_recv()
         tiny_copy(k + 1).start()
         mat_copy(k).wait_recv()
         mat_copy(k + 1).start()
-    piece_copy(evens[0]).wait_recv()
-    piece_copy(evens[0] + 1).start()
     for k in [1] + [k + 1 for k in evens]:
         tiny_copy(k).wait_recv()
         mat_copy(k).wait_recv()
@@ -285,11 +298,11 @@
         crossing(i).start()
 
     if group == 1:
-        order = [0, 1, evens[0], evens[0] + 1] + evens[1:] + [k + 1 for k in evens[1:]]
+        order = [0, 1] + evens + [k + 1 for k in evens]
         spots = [at(k) for k in order]
     else:
         order = spots = list(range(count))
-        for k in evens[1:]:
+        for k in evens:
             pass_on(k)
         for k in [1] + [k + 1 for k in evens]:
             piece_copy(k).wait_recv()
@@ -299,7 +312,7 @@
         else:
             if k % 2:
                 piece_copy(k).wait_recv()
-            elif k in evens[1:]:
+            elif k:
                 pass_on(k)
             piece = pieces[spots[i]]
         made = matmul(hid[...], piece).astype(jnp.bfloat16)
@@ -327,7 +340,165 @@
         wide = mixed_ref[:, first : first + span].astype(jnp.float32)
         normed = (wide * scale * gain_ref[:, first : first + span]).astype(jnp.bfloat16)
         picked = matmul(chosen, normed).astype(jnp.bfloat16)
-        out_ref[:, :, first : first + span] = picked.reshape(experts, padded, span)
+        x_ref[:, :, first : first + span] = picked.reshape(experts, padded, span)
+
+
+    inner = ((sp // 2 + 1) // 2) % 2
+
+    def pick(i, outer_order, inner_order):
+        if n != 8:
+            return (i + 1) % n
+        return sum(
+            jnp.where(i == j, a + inner * (b - a), 0)
+            for j, (a, b) in enumerate(zip(outer_order, inner_order))
+        )
+
+    def turn(i):
+        return pick(i, (1, 2, 3, 6, 7, 4, 5, 0), (1, 2, 4, 5, 3, 6, 7, 0))
+
+    def home_turn(i):
+        return pick(i, (1, 2, 4, 5, 6, 7, 3), (1, 2, 3, 4, 6, 5, 7))
+
+    def direct(k):
+        other = flip(sp, k, bits)
+        return remote(
+            x_ref.at[other], arrive.at[sp, tp], direct_s.at[k], direct_r.at[k], (other, tp)
+        )
+
+    def across(k, src):
+        s = flip(sp, k, bits)
+        return remote(src(s), arrive.at[s, tp], across_s.at[k], across_r.at[k], (sp, q))
+
+    def side(k, src):
+        s = flip(sp, k, bits)
+        return remote(src(s), arrive.at[s, tp], side_s.at[k], side_r.at[k], (sp, p))
+
+    def landed(s):
+        return arrive.at[s, tp]
+
+    def fresh(s):
+        return x_ref.at[s]
+
+    def relay(k):
+        s = flip(sp, k, bits)
+        return remote(
+            arrive.at[s, q], arrive.at[s, q], relay_s.at[k], relay_r.at[k], (sp, p)
+        )
+
+    def close_far(k):
+        s = flip(sp, k, bits)
+        return remote(
+            part.at[s, (p + 2) % 4], close.at[0, k], close_s.at[0, k], close_r.at[0, k], (sp, p)
+        )
+
+    def close_own(k):
+        s = flip(sp, k, bits)
+        return remote(part.at[s, p], close.at[1, k], close_s.at[1, k], close_r.at[1, k], (sp, p))
+
+    def paying(k):
+        return remote(paid.at[k], other_half.at[k], paid_s.at[k], paid_r.at[k], (sp, q))
+
+    def homeward(k):
+        other = flip(sp, k, bits)
+        return remote(result.at[k], home.at[sp], home_s.at[k], home_r.at[k], (other, tp))
+
+    for k in (1, 2, 4, 5, 6, 7, 3) if n == 8 else range(1, n):
+        direct(k).start()
+    across(0, fresh).start()
+    side(0, fresh).start()
+    arrive[sp, tp] = x_ref[sp]
+    routed[...] = mixed_ref[...].astype(jnp.float32)
+    for load in loads[3:]:
+        load.wait()
+
+    def merge(s, back):
+        coarse, fine = narrow(share_ref[s])
+        routed[...] += matmul_t(coarse, back) + matmul_t(fine, back)
+
+    def fold(i):
+        k = home_turn(i)
+        homeward(k).wait_recv()
+        s = flip(sp, k, bits)
+        merge(s, home[s])
+
+    early = min(3, n - 1)
+
+    @pl.loop(0, n + 4)
+    def _(i):
+        @pl.when(i < n - 1)
+        def _():
+            k = turn(i)
+            direct(k).wait_recv()
+            across(k, landed).start()
+            side(k, landed).start()
+
+        @pl.when((i >= 1) & (i <= n))
+        def _():
+            k = turn(i - 1)
+            across(k, landed).wait_recv()
+            relay(k).start()
+
+        @pl.when((i >= 2) & (i <= n + 1))
+        def _():
+            k = turn(i - 2)
+            s = flip(sp, k, bits)
+            side(k, landed).wait_recv()
+            relay(k).wait_recv()
+            pre = matmul(arrive[s].reshape(4 * padded, width), gate_up[...])
+            gate = pre[:, :hidden]
+            act = (gate / (1.0 + jnp.exp(-gate)) * pre[:, hidden:]).astype(jnp.bfloat16)
+            out = matmul(act, down[...])
+            part[s] = out.astype(jnp.bfloat16).reshape(4, padded, width)
+            close_far(k).start()
+            close_own(k).start()
+
+        @pl.when((i >= 3) & (i <= n + 2))
+        def _():
+            k = turn(i - 3)
+            s = flip(sp, k, bits)
+            close_far(k).wait_recv()
+            both = part[s, q].astype(jnp.float32) + close[0, k].astype(jnp.float32)
+            paid[k] = both.astype(jnp.bfloat16)
+            paying(k).start()
+
+        @pl.when(i >= 4)
+        def _():
+            k = turn(i - 4)
+            s = flip(sp, k, bits)
+            close_own(k).wait_recv()
+            paying(k).wait_recv()
+            both = part[s, tp].astype(jnp.float32) + close[1, k].astype(jnp.float32)
+            result[k] = (both + other_half[k].astype(jnp.float32)).astype(jnp.bfloat16)
+
+            @pl.when(i < n + 3)
+            def _():
+                homeward(k).start()
+
+        @pl.when((i >= 6) & (i < 6 + early))
+        def _():
+            fold(i - 6)
+
+    merge(sp, result[0])
+
+    @pl.loop(early, n - 1)
+    def _(i):
+        fold(i)
+
+    out_ref[...] = routed[...].astype(jnp.bfloat16)
+
+    @pl.loop(0, n)
+    def _(k):
+        @pl.when(k > 0)
+        def _():
+            homeward(k).wait_send()
+            direct(k).wait_send()
+
+        across(k, landed).wait_send()
+        side(k, landed).wait_send()
+        relay(k).wait_send()
+        close_far(k).wait_send()
+        close_own(k).wait_send()
+        paying(k).wait_send()
 
     for k in range(1, n):
         tiny_copy(k).wait_send()
@@ -339,7 +510,7 @@
         crossing(i).wait_send()
 
 
-def cell_stage(capacity, q, k, v, gate_in, forget, extra, residual, weight, gain, ids, wts):
+def layer(capacity, q, k, v, gate_in, forget, extra, residual, weight, gain, ids, wts, *mats):
     n = lax.axis_size("sp")
     length, channels = q.shape
     heads = gate_in.shape[0]
@@ -349,225 +520,42 @@
     chunk = max(1, 256 // columns) * columns
     count = width // chunk
     padded = -(-capacity // 8) * 8
-    vmem = pl.BlockSpec(memory_space=pltpu.VMEM)
-    dma = pltpu.SemaphoreType.DMA
-    kind = residual.dtype
-    return pl.pallas_call(
-        functools.partial(cell_kernel, n, capacity, padded),
-        out_shape=(
-            jax.ShapeDtypeStruct((n, padded, width), kind),
-            jax.ShapeDtypeStruct((rows, width), kind),
-            jax.ShapeDtypeStruct((n * padded, rows), jnp.float32),
-        ),
-        in_specs=[vmem] * 11,
-        out_specs=(vmem,) * 3,
-        scratch_shapes=[
-            pltpu.VMEM((channels, dim), kind),
-            pltpu.VMEM((n, channels, dim), kind),
-            pltpu.VMEM((8, dim), jnp.float32),
-            pltpu.VMEM((n, 8, dim), jnp.float32),
-            pltpu.VMEM((n, channels, columns), kind),
-            pltpu.VMEM((heads, length, 2 * dim), jnp.float32),
-            pltpu.VMEM((length, channels), kind),
-            pltpu.VMEM((count, length // rows, rows, chunk), kind),
-            pltpu.VMEM((2, count, rows, chunk), kind),
-            pltpu.VMEM((count, rows, chunk), kind),
-            pltpu.VMEM((count, rows, chunk), kind),
-        ]
-        + [dma((n,))] * 6
-        + [dma((2, count))] * 2
-        + [dma((count,))] * 2,
-        compiler_params=pltpu.CompilerParams(
-            collective_id=2, has_side_effects=True, vmem_limit_bytes=58 * 2**20
-        ),
-    )(q, k, v, gate_in, forget, extra, residual, weight, gain, ids, wts)
-
-
-def experts_kernel(
-    x_ref, gate_hbm, up_hbm, down_hbm, share_ref, mixed_ref, out_ref,
-    gate_up, down, arrive, part, near, sent, far, result, home,
-    weight_sems, direct_s, direct_r, across_s, across_r, side_s, side_r, relay_s, relay_r,
-    near_s, near_r, far_s, far_r, home_s, home_r,
-):
-    sp, tp, n, p, q = places()
-    bits = n.bit_length() - 1
-    half = n // 2
-    hidden = down.shape[0]
-    width = x_ref.shape[2]
-    rows = x_ref.shape[1]
-    pulls = [
-        pltpu.make_async_copy(gate_hbm.at[0], gate_up.at[:, pl.ds(0, hidden)], weight_sems.at[0]),
-        pltpu.make_async_copy(up_hbm.at[0], gate_up.at[:, pl.ds(hidden, hidden)], weight_sems.at[1]),
-        pltpu.make_async_copy(down_hbm.at[0], down, weight_sems.at[2]),
-    ]
-    for pull in pulls:
-        pull.start()
-    greet([(flip(sp, k, bits), tp) for k in range(1, n)] + [(sp, p), (sp, q)])
-
-    def turn(i):
-        late = i // half
-        return (1 - late) * (half + i) + late * (n - 1 - i)
-
-    def direct(i):
-        k = turn(i)
-        other = flip(sp, k, bits)
-        return remote(
-            x_ref.at[other], arrive.at[sp, tp], direct_s.at[i], direct_r.at[i], (other, tp)
-        )
-
-    def across(i, src):
-        s = flip(sp, turn(i), bits)
-        return remote(src(s), arrive.at[s, tp], across_s.at[i], across_r.at[i], (sp, q))
-
-    def side(i, src):
-        s = flip(sp, turn(i), bits)
-        return remote(src(s), arrive.at[s, tp], side_s.at[i], side_r.at[i], (sp, p))
-
-    def landed(s):
-        return arrive.at[s, tp]
-
-    def mine(s):
-        return x_ref.at[s]
-
-    def relay(i):
-        s = flip(sp, turn(i), bits)
-        return remote(
-            arrive.at[s, q], arrive.at[s, q], relay_s.at[i], relay_r.at[i], (sp, p)
-        )
-
-    def near_far(i):
-        s = flip(sp, turn(i), bits)
-        return remote(
-            part.at[s, (p + 2) % 4], near.at[0, i], near_s.at[0, i], near_r.at[0, i], (sp, p)
-        )
-
-    def near_own(i):
-        s = flip(sp, turn(i), bits)
-        return remote(part.at[s, p], near.at[1, i], near_s.at[1, i], near_r.at[1, i], (sp, p))
-
-    def crossing(i):
-        return remote(sent.at[i], far.at[i], far_s.at[i], far_r.at[i], (sp, q))
-
-    def homeward(i):
-        other = flip(sp, turn(i), bits)
-        return remote(result.at[i], home.at[sp], home_s.at[i], home_r.at[i], (other, tp))
-
-    @pl.loop(0, n - 1)
-    def _(i):
-        direct(i).start()
-
-    across(n - 1, mine).start()
-    side(n - 1, mine).start()
-    arrive[sp, tp] = x_ref[sp]
-    for pull in pulls:
-        pull.wait()
-
-    @pl.loop(0, n + 4)
-    def _(i):
-        @pl.when(i < n - 1)
-        def _():
-            direct(i).wait_recv()
-            across(i, landed).start()
-            side(i, landed).start()
-
-        @pl.when((i >= 1) & (i <= n))
-        def _():
-            across(i - 1, landed).wait_recv()
-            relay(i - 1).start()
-
-        @pl.when((i >= 2) & (i <= n + 1))
-        def _():
-            j = i - 2
-            s = flip(sp, turn(j), bits)
-            side(j, landed).wait_recv()
-            relay(j).wait_recv()
-            pre = jnp.dot(
-                arrive[s].reshape(4 * rows, width), gate_up[...],
-                preferred_element_type=jnp.float32,
-            )
-            gate = pre[:, :hidden]
-            act = (gate / (1.0 + jnp.exp(-gate)) * pre[:, hidden:]).astype(jnp.bfloat16)
-            out = jnp.dot(act, down[...], preferred_element_type=jnp.float32)
-            part[s] = out.astype(jnp.bfloat16).reshape(4, rows, width)
-            near_far(j).start()
-            near_own(j).start()
-
-        @pl.when((i >= 3) & (i <= n + 2))
-        def _():
-            j = i - 3
-            s = flip(sp, turn(j), bits)
-            near_far(j).wait_recv()
-            total = part[s, q].astype(jnp.float32) + near[0, j].astype(jnp.float32)
-            sent[j] = total.astype(jnp.bfloat16)
-            crossing(j).start()
-
-        @pl.when(i >= 4)
-        def _():
-            j = i - 4
-            s = flip(sp, turn(j), bits)
-            near_own(j).wait_recv()
-            crossing(j).wait_recv()
-            total = part[s, tp].astype(jnp.float32) + near[1, j].astype(jnp.float32)
-            result[j] = (total + far[j].astype(jnp.float32)).astype(jnp.bfloat16)
-
-            @pl.when(j < n - 1)
-            def _():
-                homeward(j).start()
-
-    home[sp] = result[n - 1]
-
-    @pl.loop(0, n - 1)
-    def _(i):
-        homeward(i).wait()
-        direct(i).wait_send()
-
-    @pl.loop(0, n)
-    def _(i):
-        across(i, landed).wait_send()
-        side(i, landed).wait_send()
-        relay(i).wait_send()
-        near_far(i).wait_send()
-        near_own(i).wait_send()
-        crossing(i).wait_send()
-
-    share = share_ref[...]
-    coarse, fine = narrow(share)
-    back = home[...].reshape(n * rows, width)
-    routed = matmul_t(coarse, back) + matmul_t(fine, back)
-    out_ref[...] = (mixed_ref[...].astype(jnp.float32) + routed).astype(jnp.bfloat16)
-
-
-def experts_stage(x, gate, up, down, share, mixed):
-    n, rows, width = x.shape
-    hidden = down.shape[1]
-    block = (n, rows, width)
+    hidden = mats[2].shape[1]
     vmem = pl.BlockSpec(memory_space=pltpu.VMEM)
     hbm = pl.BlockSpec(memory_space=pl.ANY)
     dma = pltpu.SemaphoreType.DMA
+    kind = residual.dtype
+    block = (n, padded, width)
+    shapes = [
+        (length, channels), (rows, width), (channels, dim), (n, channels, dim), None, None,
+        (n, channels, columns), None, (length, channels), (count, length // rows, rows, chunk),
+        (2, count, rows, chunk), (count, rows, chunk), (count, rows, chunk),
+        block, (rows, width), None, (width, 2 * hidden), (hidden, width),
+        (n, 4) + block[1:], (n, 4) + block[1:], (2,) + block, block, block, block, block, None,
+    ]
+    wide = iter(
+        [(8, dim), (n, 8, dim), (heads, length, 2 * dim), (n, padded, rows), (rows, width)]
+    )
     return pl.pallas_call(
-        experts_kernel,
-        out_shape=jax.ShapeDtypeStruct(mixed.shape, mixed.dtype),
-        in_specs=[vmem, hbm, hbm, hbm, vmem, vmem],
+        functools.partial(layer_kernel, capacity, padded),
+        out_shape=jax.ShapeDtypeStruct((rows, width), kind),
+        in_specs=[hbm] + [vmem] * 5 + [hbm] * 2 + [vmem] * 3 + [hbm] * 3,
         out_specs=vmem,
         scratch_shapes=[
-            pltpu.VMEM((width, 2 * hidden), x.dtype),
-            pltpu.VMEM((hidden, width), x.dtype),
-            pltpu.VMEM((n, 4, rows, width), x.dtype),
-            pltpu.VMEM((n, 4, rows, width), x.dtype),
-            pltpu.VMEM((2,) + block, x.dtype),
-            pltpu.VMEM(block, x.dtype),
-            pltpu.VMEM(block, x.dtype),
-            pltpu.VMEM(block, x.dtype),
-            pltpu.VMEM(block, x.dtype),
-            dma((3,)),
+            pltpu.VMEM(shape, kind) if shape else pltpu.VMEM(next(wide), jnp.float32)
+            for shape in shapes
         ]
+        + [dma((6,))]
+        + [dma((n,))] * 6
+        + [dma((2, count))] * 2
+        + [dma((count,))] * 2
         + [dma((n,))] * 8
         + [dma((2, n))] * 2
         + [dma((n,))] * 4,
         compiler_params=pltpu.CompilerParams(
-            collective_id=1, has_side_effects=True, vmem_limit_bytes=60 * 2**20
+            collective_id=1, has_side_effects=True, vmem_limit_bytes=61 * 2**20
         ),
-    )(x, gate, up, down, share, mixed)
+    )(q, k, v, gate_in, forget, extra, residual, weight, gain, ids, wts, *mats)
 
 
 def local(
@@ -593,7 +581,7 @@
     own_ids = lax.dynamic_slice_in_dim(
         routed_expert_index, lax.axis_index("tp") * row_count, row_count, 0
     )
-    outgoing, mixed, share = cell_stage(
+    return layer(
         capacity,
         memory_queries,
         memory_keys,
@@ -606,9 +594,9 @@
         expert_norm_gain[None, :],
         own_ids.T,
         routed_expert_weight.T,
-    )
-    return experts_stage(
-        outgoing, expert_gate_weight, expert_up_weight, expert_down_weight, share, mixed
+        expert_gate_weight,
+        expert_up_weight,
+        expert_down_weight,
     )
 
 

time: 136 us -> 113 us (0.83)
  the two profiles are of different devices: /device:TPU:0 before, /device:TPU:12 now
where the time goes in v3:
time: 113 us
  Pallas kernels  110 us (97%)
  local copies, waits for them, and re-layouts  3.13 us (3%)
    pallas_call x1, Pallas kernels, layer(): pl.pallas_call(functools.partial(layer_kernel, capacity, padded), out_sha...  110 us
    unnamed x3, local copies, waits for them, and re-layouts  2.57 us

profile of v3, /device:TPU:12, one launch (start us, length us, event | category | flops | bytes accessed | tf_op | source)
XLA Modules:
  0.0 112.8 jit_solution(12315377302434652068)
XLA Ops:
  0.0 0.0 copy-start
  0.0 0.7 copy-done
  0.7 0.6 dynamic-slice_bitcast_fusion.ids_ref
  1.3 109.7 %shard_map.136 = bf16[128,2048]{1,0:T(8,128)(2,1)} custom-call(bf16[512,256]{1,0:T(8,128)(2,1)} %q_hbm.1, bf16[512,256]{1,0:T(8,128)(2,1)} %k_ref.1, bf16[512,256]{1,0:T(8,128)(2,1)} %v_ref.1, f32[2,512]{1,0:T(2,128)} %in_ref.1, f32[2,512]{1,0:T(2,128)} %forget_ref.1, f32[2,512]{1,0:T(2,128)} %extra_ref.1, bf16[128,2048]{1,0:T(8,128)(2,1)} %res_hbm.1, ...), custom_call_target="tpu_custom_call" | custom-call | tf_op jit(solution)/shard_map/pallas_call | solution.py:539
  110.9 1.9 %copy.16 = bf16[128,2048]{1,0:T(8,128)(2,1)} copy(bf16[128,2048]{1,0:T(8,128)(2,1)} %shard_map.136) | data formatting | bytes 1048576
Async XLA Ops:
  0.0 0.7 copy-start

commit v4 on v3

--- a/solution.py
+++ b/solution.py
@@ -111,12 +111,12 @@
 
 def layer_kernel(
     capacity, padded,
-    q_hbm, k_ref, v_ref, in_ref, forget_ref, extra_ref, res_hbm, w_hbm, gain_ref, ids_ref, wts_ref,
+    q_hbm, k_hbm, v_hbm, in_hbm, forget_hbm, extra_hbm, res_hbm, w_hbm, gain_hbm, ids_hbm, wts_hbm,
     gate_hbm, up_hbm, down_hbm, out_ref,
-    q_ref, res_ref, mine, mats, tiny_mine, tiny, pieces, pairs, hid, partial, near, sent, far,
+    k_ref, v_ref, in_ref, forget_ref, extra_ref, gain_ref, ids_ref, wts_ref, q_ref, res_ref, mine, mats, tiny_mine, tiny, pieces, pairs, hid, partial, near, sent, far,
     x_ref, mixed_ref, share_ref, gate_up, down, arrive, part, close, paid, other_half, result,
     home, routed,
-    load_sems, mat_s, mat_r, tiny_s, tiny_r, piece_s, piece_r, near_s, near_r, far_s, far_r,
+    load_sems, early_sems, mat_s, mat_r, tiny_s, tiny_r, piece_s, piece_r, near_s, near_r, far_s, far_r,
     direct_s, direct_r, across_s, across_r, side_s, side_r, relay_s, relay_r,
     close_s, close_r, paid_s, paid_r, home_s, home_r,
 ):
@@ -129,6 +129,9 @@
     columns = pieces.shape[2]
     hidden = down.shape[0]
     experts = n
+    group = max(1, 256 // columns)
+    chunk = group * columns
+    count = width // chunk
     count_greeted = announce([(flip(sp, k, bits), tp) for k in range(1, n)] + [(sp, p), (sp, q)])
     loads = [
         pltpu.make_async_copy(w_hbm, pieces.at[sp], load_sems.at[0]),
@@ -138,8 +141,20 @@
         pltpu.make_async_copy(up_hbm.at[0], gate_up.at[:, pl.ds(hidden, hidden)], load_sems.at[4]),
         pltpu.make_async_copy(down_hbm.at[0], down, load_sems.at[5]),
     ]
-    for load in loads:
+    early_loads = [
+        pltpu.make_async_copy(src, dst, early_sems.at[j])
+        for j, (src, dst) in enumerate(
+            [
+                (forget_hbm, forget_ref), (extra_hbm, extra_ref), (in_hbm, in_ref),
+                (k_hbm, k_ref), (v_hbm, v_ref),
+                (ids_hbm, ids_ref), (wts_hbm, wts_ref), (gain_hbm, gain_ref),
+            ]
+        )
+    ]
+    for load in early_loads + loads[:3]:
         load.start()
+    for load in early_loads:
+        load.wait()
     evens = list(range(2, n, 2))
 
     def at(k):
@@ -162,6 +177,10 @@
         src = pieces.at[slot]
         to = at(1) if k % 2 else at(k)
         return remote(src, pieces.at[slot], piece_s.at[k], piece_r.at[k], (to, tp))
+
+    def pass_on(k):
+        piece_copy(k).wait_recv()
+        piece_copy(k + 1).start()
 
     logits = forget_ref[...]
     log_forget = (
@@ -198,6 +217,8 @@
     loads[0].wait()
     for k in [1] + evens:
         piece_copy(k).start()
+    for load in loads[3:]:
+        load.start()
     mats[sp] = mine[...]
     tiny[sp] = tiny_mine[...]
     loads[1].wait()
@@ -220,7 +241,8 @@
             coarse, fine = narrow(scores)
             pairs[h, first:end] = matmul(coarse, widened[:end]) + matmul(fine, widened[:end])
 
-    chosen, share = slot_tables(ids_ref[...], wts_ref[...], experts, capacity, padded)
+    ids = ids_ref[:, pl.ds(pl.multiple_of(tp * rows, rows), rows)]
+    chosen, share = slot_tables(ids, wts_ref[...], experts, capacity, padded)
     share_ref[...] = share.reshape(experts, padded, rows)
     loads[2].wait()
 
@@ -229,6 +251,8 @@
         tiny_copy(k + 1).start()
         mat_copy(k).wait_recv()
         mat_copy(k + 1).start()
+    if group == 1:
+        pass_on(2)
     for k in [1] + [k + 1 for k in evens]:
         tiny_copy(k).wait_recv()
         mat_copy(k).wait_recv()
@@ -272,14 +296,6 @@
         )
         hid[:, lanes] = (both[:, :dim] / guard).astype(jnp.bfloat16)
 
-    group = max(1, 256 // columns)
-    chunk = group * columns
-    count = width // chunk
-
-    def pass_on(k):
-        piece_copy(k).wait_recv()
-        piece_copy(k + 1).start()
-
     def near_far(i):
         return remote(
             partial.at[i, (p + 2) % 4], near.at[0, i], near_s.at[0, i], near_r.at[0, i], (sp, p)
@@ -297,8 +313,79 @@
         sent[i] = both.astype(jnp.bfloat16)
         crossing(i).start()
 
+    inner = ((sp // 2 + 1) // 2) % 2
+
+    def pick(i, outer_order, inner_order):
+        if n != 8:
+            return (i + 1) % n
+        return sum(
+            jnp.where(i == j, a + inner * (b - a), 0)
+            for j, (a, b) in enumerate(zip(outer_order, inner_order))
+        )
+
+    def turn(i):
+        return pick(i, (1, 2, 3, 6, 7, 4, 5, 0), (1, 2, 4, 5, 3, 6, 7, 0))
+
+    def home_turn(i):
+        return pick(i, (1, 2, 4, 5, 6, 7, 3), (1, 2, 3, 4, 6, 5, 7))
+
+    def span(s, h):
+        first = s // (n // 2) if group == 1 else 0
+        return pl.ds(pl.multiple_of((first + h) % 2 * (width // 2), width // 2), width // 2)
+
+    def landed(s, h):
+        return arrive.at[s, tp, :, span(s, h)]
+
+    def fresh(s, h):
+        return x_ref.at[s, :, span(s, h)]
+
+    def direct(k, h):
+        other = flip(sp, k, bits)
+        return remote(
+            x_ref.at[other, :, span(sp, h)], landed(sp, h),
+            direct_s.at[h, k], direct_r.at[h, k], (other, tp),
+        )
+
+    def across(k, h, src=landed):
+        s = flip(sp, k, bits)
+        return remote(src(s, h), landed(s, h), across_s.at[h, k], across_r.at[h, k], (sp, q))
+
+    def side(k, h, src=landed):
+        s = flip(sp, k, bits)
+        return remote(src(s, h), landed(s, h), side_s.at[h, k], side_r.at[h, k], (sp, p))
+
+    def relay(k, h):
+        s = flip(sp, k, bits)
+        block = arrive.at[s, q, :, span(s, h)]
+        return remote(block, block, relay_s.at[h, k], relay_r.at[h, k], (sp, p))
+
+    def take(i, h):
+        k = turn(i)
+        direct(k, h).wait_recv()
+        across(k, h).start()
+        side(k, h).start()
+
+    def finish(i):
+        near_own(i).wait_recv()
+        crossing(i).wait_recv()
+        where = pl.ds(pl.multiple_of(spots[i] * chunk, chunk), chunk)
+        both = partial[i, tp].astype(jnp.float32) + near[1, i].astype(jnp.float32)
+        both = both + far[i].astype(jnp.float32)
+        mixed = res_ref[:, where].astype(jnp.float32) + both
+        mixed_ref[:, where] = mixed.astype(jnp.bfloat16)
+
+    def publish(h):
+        where = span(sp, h)
+        picked = matmul(chosen, mixed_ref[:, where]).astype(jnp.bfloat16)
+        x_ref[:, :, where] = picked.reshape(experts, padded, width // 2)
+        for k in (1, 2, 4, 5, 6, 7, 3) if n == 8 else range(1, n):
+            direct(k, h).start()
+        across(0, h, fresh).start()
+        side(0, h, fresh).start()
+
+
     if group == 1:
-        order = [0, 1] + evens + [k + 1 for k in evens]
+        order = [0, 1] + evens[:1] + [3] + evens[1:] + [k + 1 for k in evens[1:]]
         spots = [at(k) for k in order]
     else:
         order = spots = list(range(count))
@@ -307,13 +394,14 @@
         for k in [1] + [k + 1 for k in evens]:
             piece_copy(k).wait_recv()
     for i, k in enumerate(order):
+        if i == 3 and group == 1:
+            for even in evens[1:]:
+                pass_on(even)
         if group > 1:
             piece = jnp.concatenate([pieces[i * group + j] for j in range(group)], axis=1)
         else:
             if k % 2:
                 piece_copy(k).wait_recv()
-            elif k:
-                pass_on(k)
             piece = pieces[spots[i]]
         made = matmul(hid[...], piece).astype(jnp.bfloat16)
         partial[i] = made.reshape(length // rows, rows, chunk)
@@ -321,69 +409,21 @@
         near_own(i).start()
         if i:
             cross(i - 1)
+        if i == count // 2:
+            for j in range(i):
+                finish(j)
+            publish(0)
     cross(count - 1)
-
-    squares = jnp.zeros((rows, 1), jnp.float32)
-    for i in range(count):
-        near_own(i).wait_recv()
-        crossing(i).wait_recv()
-        where = pl.ds(pl.multiple_of(spots[i] * chunk, chunk), chunk)
-        both = partial[i, tp].astype(jnp.float32) + near[1, i].astype(jnp.float32)
-        both = both + far[i].astype(jnp.float32)
-        mixed = (res_ref[:, where].astype(jnp.float32) + both).astype(jnp.bfloat16)
-        mixed_ref[:, where] = mixed
-        wide = mixed.astype(jnp.float32)
-        squares = squares + jnp.sum(wide * wide, axis=1, keepdims=True)
-    scale = lax.rsqrt(squares / width + epsilon)
-    span = min(width, 512)
-    for first in range(0, width, span):
-        wide = mixed_ref[:, first : first + span].astype(jnp.float32)
-        normed = (wide * scale * gain_ref[:, first : first + span]).astype(jnp.bfloat16)
-        picked = matmul(chosen, normed).astype(jnp.bfloat16)
-        x_ref[:, :, first : first + span] = picked.reshape(experts, padded, span)
-
-
-    inner = ((sp // 2 + 1) // 2) % 2
-
-    def pick(i, outer_order, inner_order):
-        if n != 8:
-            return (i + 1) % n
-        return sum(
-            jnp.where(i == j, a + inner * (b - a), 0)
-            for j, (a, b) in enumerate(zip(outer_order, inner_order))
-        )
-
-    def turn(i):
-        return pick(i, (1, 2, 3, 6, 7, 4, 5, 0), (1, 2, 4, 5, 3, 6, 7, 0))
-
-    def home_turn(i):
-        return pick(i, (1, 2, 4, 5, 6, 7, 3), (1, 2, 3, 4, 6, 5, 7))
-
-    def direct(k):
-        other = flip(sp, k, bits)
-        return remote(
-            x_ref.at[other], arrive.at[sp, tp], direct_s.at[k], direct_r.at[k], (other, tp)
-        )
-
-    def across(k, src):
-        s = flip(sp, k, bits)
-        return remote(src(s), arrive.at[s, tp], across_s.at[k], across_r.at[k], (sp, q))
-
-    def side(k, src):
-        s = flip(sp, k, bits)
-        return remote(src(s), arrive.at[s, tp], side_s.at[k], side_r.at[k], (sp, p))
-
-    def landed(s):
-        return arrive.at[s, tp]
-
-    def fresh(s):
-        return x_ref.at[s]
-
-    def relay(k):
-        s = flip(sp, k, bits)
-        return remote(
-            arrive.at[s, q], arrive.at[s, q], relay_s.at[k], relay_r.at[k], (sp, p)
-        )
+    for j in range(count // 2, count):
+        finish(j)
+        if j == count - 4:
+            take(0, 0)
+        if j == count - 2:
+            take(1, 0)
+    publish(1)
+    lead = 4
+    take(2, 0)
+    take(3, 0)
 
     def close_far(k):
         s = flip(sp, k, bits)
@@ -402,10 +442,6 @@
         other = flip(sp, k, bits)
         return remote(result.at[k], home.at[sp], home_s.at[k], home_r.at[k], (other, tp))
 
-    for k in (1, 2, 4, 5, 6, 7, 3) if n == 8 else range(1, n):
-        direct(k).start()
-    across(0, fresh).start()
-    side(0, fresh).start()
     arrive[sp, tp] = x_ref[sp]
     routed[...] = mixed_ref[...].astype(jnp.float32)
     for load in loads[3:]:
@@ -427,24 +463,29 @@
     def _(i):
         @pl.when(i < n - 1)
         def _():
-            k = turn(i)
-            direct(k).wait_recv()
-            across(k, landed).start()
-            side(k, landed).start()
+            take(i, 1)
+
+        @pl.when(i < n - 1 - lead)
+        def _():
+            take(i + lead, 0)
 
         @pl.when((i >= 1) & (i <= n))
         def _():
             k = turn(i - 1)
-            across(k, landed).wait_recv()
-            relay(k).start()
+            for h in range(2):
+                across(k, h).wait_recv()
+                relay(k, h).start()
 
         @pl.when((i >= 2) & (i <= n + 1))
         def _():
             k = turn(i - 2)
             s = flip(sp, k, bits)
-            side(k, landed).wait_recv()
-            relay(k).wait_recv()
-            pre = matmul(arrive[s].reshape(4 * padded, width), gate_up[...])
+            for h in range(2):
+                side(k, h).wait_recv()
+                relay(k, h).wait_recv()
+            wide = arrive[s].reshape(4 * padded, width).astype(jnp.float32)
+            scale = lax.rsqrt(jnp.mean(wide * wide, axis=1, keepdims=True) + epsilon)
+            pre = matmul((wide * scale * gain_ref[...]).astype(jnp.bfloat16), gate_up[...])
             gate = pre[:, :hidden]
             act = (gate / (1.0 + jnp.exp(-gate)) * pre[:, hidden:]).astype(jnp.bfloat16)
             out = matmul(act, down[...])
@@ -461,6 +502,11 @@
             paid[k] = both.astype(jnp.bfloat16)
             paying(k).start()
 
+        @pl.when(i == n + 3)
+        def _():
+            for f in range(early, min(early + 2, n - 1)):
+                fold(f)
+
         @pl.when(i >= 4)
         def _():
             k = turn(i - 4)
@@ -480,7 +526,7 @@
 
     merge(sp, result[0])
 
-    @pl.loop(early, n - 1)
+    @pl.loop(min(early + 2, n - 1), n - 1)
     def _(i):
         fold(i)
 
@@ -491,11 +537,13 @@
         @pl.when(k > 0)
         def _():
             homeward(k).wait_send()
-            direct(k).wait_send()
-
-        across(k, landed).wait_send()
-        side(k, landed).wait_send()
-        relay(k).wait_send()
+            for h in range(2):
+                direct(k, h).wait_send()
+
+        for h in range(2):
+            across(k, h).wait_send()
+            side(k, h).wait_send()
+            relay(k, h).wait_send()
         close_far(k).wait_send()
         close_own(k).wait_send()
         paying(k).wait_send()
@@ -522,7 +570,7 @@
     padded = -(-capacity // 8) * 8
     hidden = mats[2].shape[1]
     vmem = pl.BlockSpec(memory_space=pltpu.VMEM)
-    hbm = pl.BlockSpec(memory_space=pl.ANY)
+    hbm = pl.BlockSpec(memory_space=pltpu.HBM)
     dma = pltpu.SemaphoreType.DMA
     kind = residual.dtype
     block = (n, padded, width)
@@ -539,18 +587,21 @@
     return pl.pallas_call(
         functools.partial(layer_kernel, capacity, padded),
         out_shape=jax.ShapeDtypeStruct((rows, width), kind),
-        in_specs=[hbm] + [vmem] * 5 + [hbm] * 2 + [vmem] * 3 + [hbm] * 3,
+        in_specs=[hbm] * 14,
         out_specs=vmem,
         scratch_shapes=[
+            pltpu.VMEM(ref.shape, ref.dtype)
+            for ref in (k, v, gate_in, forget, extra, gain, ids, wts)
+        ]
+        + [
             pltpu.VMEM(shape, kind) if shape else pltpu.VMEM(next(wide), jnp.float32)
             for shape in shapes
         ]
-        + [dma((6,))]
+        + [dma((6,)), dma((8,))]
         + [dma((n,))] * 6
         + [dma((2, count))] * 2
         + [dma((count,))] * 2
-        + [dma((n,))] * 8
-        + [dma((2, n))] * 2
+        + [dma((2, n))] * 10
         + [dma((n,))] * 4,
         compiler_params=pltpu.CompilerParams(
             collective_id=1, has_side_effects=True, vmem_limit_bytes=61 * 2**20
@@ -578,9 +629,6 @@
     experts = lax.axis_size("sp") * expert_gate_weight.shape[0]
     assigned = row_count * routed_expert_index.shape[1]
     capacity = max(2, assigned * 5 // (4 * experts))
-    own_ids = lax.dynamic_slice_in_dim(
-        routed_expert_index, lax.axis_index("tp") * row_count, row_count, 0
-    )
     return layer(
         capacity,
         memory_queries,
@@ -592,7 +640,7 @@
         residual,
         cell_output_weight,
         expert_norm_gain[None, :],
-        own_ids.T,
+        routed_expert_index.T,
         routed_expert_weight.T,
         expert_gate_weight,
         expert_up_weight,

time: 113 us -> 110 us (0.973)
  Pallas kernels: 110 us -> 108 us
  local copies, waits for them, and re-layouts: 3.13 us -> 1.88 us
    pallas_call x1, Pallas kernels: 110 us -> 108 us  [layer(): pl.pallas_call(functools.partial(layer_kernel, capacity, padded), out_sha...]
    unnamed x3 -> x1, local copies, waits for them, and re-layouts: 2.57 us -> 1.88 us
where the time goes in v4:
time: 110 us; the launch traced here: 109 us
  Pallas kernels  108 us (98%)
  local copies, waits for them, and re-layouts  1.88 us (2%)
    pallas_call x1, Pallas kernels, layer(): pl.pallas_call(functools.partial(layer_kernel, capacity, padded), out_sha...  108 us

profile of v4, /device:TPU:12, one launch (start us, length us, event | category | flops | bytes accessed | tf_op | source)
XLA Modules:
  0.0 109.4 jit_solution(2577705055461286962)
XLA Ops:
  0.0 107.5 %shard_map.136 = bf16[128,2048]{1,0:T(8,128)(2,1)} custom-call(bf16[512,256]{1,0:T(8,128)(2,1)} %q_hbm.1, bf16[512,256]{1,0:T(8,128)(2,1)} %k_hbm.1, bf16[512,256]{1,0:T(8,128)(2,1)} %v_hbm.1, f32[2,512]{1,0:T(2,128)} %in_hbm.1, f32[2,512]{1,0:T(2,128)} %forget_hbm.1, f32[2,512]{1,0:T(2,128)} %extra_hbm.1, bf16[128,2048]{1,0:T(8,128)(2,1)} %res_hbm.1, ...), custom_call_target="tpu_custom_call" | custom-call | tf_op jit(solution)/shard_map/pallas_call | solution.py:587
  107.5 1.9 %copy.16 = bf16[128,2048]{1,0:T(8,128)(2,1)} copy(bf16[128,2048]{1,0:T(8,128)(2,1)} %shard_map.136) | data formatting | bytes 1048576
